TPU v7x, 512 devices: a whole 4x8x8 slice. The times are simulated.
512 devices in a mesh: sp: 32 (over z, x), tp: 16 (over y, core).
Axes of the slice: x: 4, y: 8, z: 8, core: 2. Of those that a mesh axis runs over, the one named last changes fastest.
Arguments:
- in_gate: bfloat16 [1024, 8192], P('tp', 'sp'), may hold values from -6 to 6
- out_gate: bfloat16 [1024, 8192], P('tp', 'sp'), may hold values from -6 to 6
- values: bfloat16 [1024, 8192], P('tp', 'sp'), may hold values from -6 to 6
- conv_taps: bfloat16 [3, 1024], P(None, 'tp'), may hold values from -3.5 to 3.5
- doc_ids: int32 [8192], P('sp'), may hold values from 0 to 7, as said below
- residual: bfloat16 [8192, 2048], P('sp'), may hold values from -6 to 6
- out_weight: bfloat16 [1024, 2048], P('tp'), may hold values from -0.1875 to 0.1875
- norm_gain: bfloat16 [2048], replicated, may hold values from 0.099609375 to 1.8984375
- routes: int32 [8192, 2], P('sp'), may hold values from 0 to 31, all different within a row; in each aligned block of 256 rows (0 to 255, 256 to 511, ...) at most 24 rows name the same one
- route_weights: float32 [8192, 2], P('sp'), may hold values from 0.2 to 1
- expert_gate: bfloat16 [32, 2048, 4224], P('sp', None, 'tp'), may hold values from -0.125 to 0.125
- expert_up: bfloat16 [32, 2048, 4224], P('sp', None, 'tp'), may hold values from -0.125 to 0.125
- expert_down: bfloat16 [32, 4224, 2048], P('sp', 'tp'), may hold values from -0.09375 to 0.09375
Outputs:
- merged: bfloat16 [8192, 2048], P('sp', 'tp')
Inputs may be any that keep to these rules, and one draw needn't show every extreme that they name: `routes`: each row names 2 different experts. Within the rows of one index of sp (aligned blocks of 256 rows) no expert is named more than 24 times, a bound that some expert reaches in some blocks. `doc_ids`: never falls along the sequence; starts at 0 and rises by one at each of 7 document starts, each number used.
All inputs are finite; a program needn't handle non-finite values.
Results may differ from a plain program's by a relative error of at most 0.019.
Values may be sent and summed in bfloat16 or wider, within the bound.
A program may use at most 64 MiB of HBM per device.

v0:
```python
import jax
import jax.numpy as jnp
from jax import lax
from jax.sharding import PartitionSpec as P

EPSILON = 1e-06


def shifted(x, axis, by):
    count = lax.axis_size(axis)
    pairs = [(i, i + by) for i in range(count) if 0 <= i + by < count]
    return lax.ppermute(x, axis, pairs)


def in_blocks(x, dim, count):
    before, after = (x.shape[:dim], x.shape[dim + 1 :])
    return jnp.moveaxis(x.reshape(*before, count, -1, *after), dim, 0)


def sum_at_owner(x, axis, dim):
    count = lax.axis_size(axis)
    parts = lax.all_to_all(in_blocks(x, dim, count), axis, 0, 0, tiled=True)
    return jnp.sum(parts.astype(jnp.float32), axis=0)


def copy_for_each(x, axis):
    copies = jnp.broadcast_to(x, (lax.axis_size(axis), *x.shape))
    return lax.all_to_all(copies, axis, split_axis=0, concat_axis=0, tiled=True)


def taken_together(x, axis):
    everything = copy_for_each(x, axis)
    return jnp.sum(everything, axis=0)


def shards(
    in_gate,
    out_gate,
    values,
    conv_taps,
    doc_ids,
    residual,
    out_weight,
    norm_gain,
    routes,
    route_weights,
    expert_gate,
    expert_up,
    expert_down,
):
    gated_in = (in_gate.astype(jnp.float32) * values.astype(jnp.float32)).astype(jnp.bfloat16)
    tail_rows, tail_docs = shifted((gated_in[:, -2:], doc_ids[-2:]), "sp", 1)
    extended = lax.optimization_barrier(jnp.concatenate([tail_rows, gated_in], axis=1)).astype(
        jnp.float32
    )
    docs_ext = jnp.concatenate([tail_docs, doc_ids])
    length = doc_ids.shape[0]
    near_mask = (docs_ext[1 : length + 1] == doc_ids).astype(jnp.float32)
    far_mask = (docs_ext[0:length] == doc_ids).astype(jnp.float32)
    tap_values = conv_taps.astype(jnp.float32)
    convolved = (
        tap_values[2][:, None] * extended[:, 2:]
        + tap_values[1][:, None] * extended[:, 1 : length + 1] * near_mask[None, :]
        + tap_values[0][:, None] * extended[:, 0:length] * far_mask[None, :]
    )
    mixed_rows = (out_gate.astype(jnp.float32) * convolved).astype(jnp.bfloat16)
    partial_value = lax.dot_general(
        mixed_rows, out_weight, (((0,), (0,)), ((), ())), preferred_element_type=jnp.float32
    )
    tp_count = lax.axis_size("tp")
    model_width = residual.shape[1]
    share_width = model_width // tp_count
    column = lax.axis_index("tp") * share_width
    share_sum = sum_at_owner(partial_value.astype(jnp.bfloat16), "tp", 1)
    stream_cols = (
        lax.dynamic_slice_in_dim(residual, column, share_width, 1).astype(jnp.float32) + share_sum
    )
    square_total = taken_together(jnp.sum(stream_cols * stream_cols, axis=1, keepdims=True), "tp")
    inv_rms = lax.rsqrt(square_total / model_width + EPSILON)
    gain_cols = lax.dynamic_slice_in_dim(norm_gain, column, share_width, 0).astype(jnp.float32)
    own_cols = (stream_cols * inv_rms * gain_cols[None, :]).astype(jnp.bfloat16)
    tokens = routes.shape[0]
    top_count = routes.shape[1]
    experts = lax.axis_size("sp")
    capacity = 3 * tokens * top_count // (2 * experts)
    chosen = routes.reshape(-1)
    hits_table = (chosen[:, None] == jnp.arange(experts, dtype=jnp.int32)[None, :]).astype(
        jnp.int32
    )
    earlier = jnp.cumsum(hits_table, axis=0) - hits_table
    ranked = jnp.sum(earlier * hits_table, axis=1)
    slot_index = chosen * capacity + ranked
    owners = jnp.arange(tokens * top_count, dtype=jnp.int32) // top_count
    source = jnp.zeros((experts * capacity,), jnp.int32).at[slot_index].set(owners)
    filled = jnp.zeros((experts * capacity,), jnp.bool_).at[slot_index].set(True)
    gate_weight = expert_gate[0]
    up_weight = expert_up[0]
    down_weight = expert_down[0]
    picked = jnp.where(
        filled[:, None], jnp.take(own_cols, source, axis=0), jnp.zeros((), jnp.bfloat16)
    ).reshape(experts, capacity, share_width)
    arrived = lax.all_to_all(picked, "sp", split_axis=0, concat_axis=0, tiled=True)
    slot_count = arrived.shape[1]
    row_block = arrived.reshape(-1, share_width)
    piece_cols = lax.all_gather(row_block, "tp", axis=1, tiled=True)
    gate_sum = jnp.dot(piece_cols, gate_weight, preferred_element_type=jnp.float32)
    up_sum = jnp.dot(piece_cols, up_weight, preferred_element_type=jnp.float32)
    hidden = (jax.nn.silu(gate_sum) * up_sum).astype(jnp.bfloat16)
    down_sum = jnp.dot(hidden, down_weight, preferred_element_type=jnp.float32)
    summed = lax.psum_scatter(down_sum.astype(jnp.bfloat16), "tp", scatter_dimension=1, tiled=True)
    returned = lax.all_to_all(
        summed.reshape(experts, slot_count, share_width),
        "sp",
        split_axis=0,
        concat_axis=0,
        tiled=True,
    )
    results = jnp.take(returned.reshape(experts * capacity, share_width), slot_index, axis=0)
    results = results.astype(jnp.float32).reshape(tokens, top_count, share_width)
    blended = jnp.sum(route_weights[:, :, None] * results, axis=1)
    return (stream_cols + blended).astype(jnp.bfloat16)


def solution(mesh):
    placed = (
        P("tp", "sp"),
        P("tp", "sp"),
        P("tp", "sp"),
        P(None, "tp"),
        P("sp"),
        P("sp", None),
        P("tp", None),
        P(),
        P("sp", None),
        P("sp", None),
        P("sp", None, "tp"),
        P("sp", None, "tp"),
        P("sp", "tp", None),
    )
    return jax.shard_map(
        shards, mesh=mesh, in_specs=placed, out_specs=P("sp", "tp"), check_vma=False
    )
```

profile of v0, /device:TPU:25, one launch (start us, length us, event | category | flops | bytes accessed | tf_op | source)
XLA Modules:
  0.0 249.0 jit_solution(15345662534989394620)
XLA Ops:
  6.5 0.0 copy-start
  6.5 0.9 multiply_convert_fusion.1
  7.4 0.1 slice.52
  7.5 3.1 %collective-permute-start = (bf16[64,2]{1,0:T(8,128)(2,1)S(1)}, bf16[64,2]{1,0:T(8,128)(2,1)S(1)}, u32[]{:S(2)}, u32[]{:S(2)}) collective-permute-start(bf16[64,2]{1,0:T(8,128)(2,1)S(1)} %slice.52), channel_id=1, source_target_pairs={{0,16},{16,32},{32,48},{48,64},{64,80},{80,96},{96,112},{112,128},... | collective-permute-start | bytes 776 | tf_op jit(solution)/shard_map/ppermute | solution.py:12
  10.6 0.8 slice.41
  11.4 3.1 %collective-permute-start.1 = (s32[2]{0:T(128)S(1)}, s32[2]{0:T(128)S(1)}, u32[]{:S(2)}, u32[]{:S(2)}) collective-permute-start(s32[2]{0:T(128)S(1)} %slice.41), channel_id=1, source_target_pairs={{0,16},{16,32},{32,48},{48,64},{64,80},{80,96},{96,112},{112,128},... | collective-permute-start | bytes 32 | tf_op jit(solution)/shard_map/ppermute | solution.py:12
  14.5 0.7 convert_element_type.64
  15.2 0.0 collective-permute-done.1
  15.2 0.8 pad_add_fusion
  15.9 0.8 compare_convert_fusion.1
  16.7 0.0 collective-permute-done
  16.7 0.1 pad_maximum_fusion
  16.8 1.5 fusion
  18.3 0.0 copy-start.1
  18.3 1.3 copy.41
  19.6 8.7 %all-to-all-start = ((bf16[16,256,128]{2,1,0:T(8,128)(2,1)}), bf16[16,256,128]{2,1,0:T(8,128)(2,1)S(1)}, u32[]{:S(2)}, u32[]{:S(2)}) async-start(bf16[16,256,128]{2,1,0:T(8,128)(2,1)} %bitcast.55), calls=%async_computation | async-start | bytes 2097152 | tf_op jit(solution)/shard_map/all_to_all | solution.py:22
  28.4 0.0 copy-done.1
  28.4 0.1 copy.29
  28.5 0.1 eq.34
  28.6 0.1 reshape.109
  28.8 1.2 reduce-window.6
  30.0 0.2 slice_reduce_fusion
  30.2 0.1 copy.34
  30.4 0.1 mul.131
  30.6 0.1 fusion.14
  30.7 2.4 scatter_custom_fusion.1
  33.2 0.0 copy-start.3
  33.2 21.4 %all-to-all-done = bf16[16,256,128]{2,1,0:T(8,128)(2,1)S(1)} async-done(((bf16[16,256,128]{2,1,0:T(8,128)(2,1)}), bf16[16,256,128]{2,1,0:T(8,128)(2,1)S(1)}, u32[]{:S(2)}, u32[]{:S(2)}) %all-to-all-start) | async-done | bytes 1048608 | tf_op jit(solution)/shard_map/all_to_all | solution.py:22
  54.6 0.1 convert_reduce_fusion
  54.7 1.0 multiply_reduce_fusion.1
  55.7 0.6 broadcast_in_dim.67
  56.3 5.2 %all-to-all-start.1 = ((f32[16,256,1]{1,2,0:T(1,128)}), f32[16,256,1]{1,2,0:T(1,128)S(1)}, u32[]{:S(2)}, u32[]{:S(2)}) async-start(f32[16,256,1]{1,2,0:T(1,128)} %broadcast_in_dim.67), calls=%async_computation.1 | async-start | bytes 32768 | tf_op jit(solution)/shard_map/all_to_all | solution.py:28
  61.5 0.0 all-gather.2.cloned.1.call-start
  61.5 0.8 dynamic-slice_convert_fusion
  62.3 0.1 broadcast_in_dim.65
  62.4 2.4 scatter_custom_fusion
  64.9 0.1 broadcast_in_dim.62
  65.0 1.1 all-to-all-done.1
  66.1 0.9 multiply_convert_fusion
  67.0 1.9 gather_fusion
  68.9 0.3 select_select_fusion
  69.2 25.0 %all_to_all.20 = bf16[32,24,128]{2,1,0:T(8,128)(2,1)} all-to-all(bf16[32,24,128]{2,1,0:T(8,128)(2,1)S(1)} %select_select_fusion), channel_id=1, replica_groups=mesh['sp'=32,'tp'=16] {'sp'}, dimensions={0} | all-to-all | bytes 393216 | tf_op jit(solution)/shard_map/all_to_all | solution.py:102
  94.2 0.0 all-gather.2.cloned.1.call-update
  94.2 0.0 copy-start.4
  94.2 0.0 reduce-scatter.4.cloned.1.call-start
  94.3 41.9 %all-gather.2.cloned.1.call-done = bf16[768,2048]{1,0:T(8,128)(2,1)} async-done(((bf16[768,128]{1,0:T(8,128)(2,1)}), bf16[768,2048]{1,0:T(8,128)(2,1)}) %all-gather.2.cloned.1.call-update) | async-done | bytes 3145744 | tf_op jit(solution)/shard_map/all_gather | solution.py:105
  136.1 0.0 copy-done.3
  136.2 3.8 %fusion.4 = f32[768,264]{0,1:T(8,128)} fusion(bf16[768,2048]{1,0:T(8,128)(2,1)} %all-gather.2.cloned.1.call-done, bf16[1,2048,264]{1,2,0:T(8,128)(2,1)S(1)} %copy-done.3), kind=kOutput, calls=%fused_computation.12 | convolution fusion | flops 830472192 | bytes 5038080 | tf_op jit(solution)/shard_map/dot_general | solution.py:106
  140.0 0.0 copy-done
  140.0 0.0 copy-done.4
  140.0 7.3 %convolution_convert_fusion = bf16[768,2048]{1,0:T(8,128)(2,1)} fusion(bf16[1,264,2048]{2,1,0:T(8,128)(2,1)S(1)} %copy-done, bf16[768,2048]{1,0:T(8,128)(2,1)} %all-gather.2.cloned.1.call-done, bf16[1,2048,264]{1,2,0:T(8,128)(2,1)S(1)} %copy-done.4, f32[768,264]{0,1:T(8,128)} %fusion.4), kind=kOutput, calls=%fused_computation.4 | convolution fusion | flops 1663733760 | bytes 9265152 | tf_op jit(solution)/shard_map/dot_general | solution.py:109
  147.3 4.6 %copy.35 = bf16[768,2048]{0,1:T(8,128)(2,1)} copy(bf16[768,2048]{1,0:T(8,128)(2,1)} %convolution_convert_fusion) | data formatting | bytes 6291456
  151.9 0.0 reduce-scatter.4.cloned.1.call-update
  152.0 64.2 %reduce-scatter.4.cloned.1.call-done = bf16[128,768]{1,0:T(8,128)(2,1)} async-done(((bf16[2048,768]{1,0:T(8,128)(2,1)}), bf16[128,768]{1,0:T(8,128)(2,1)}) %reduce-scatter.4.cloned.1.call-update) | async-done | bytes 196624
  216.1 1.7 copy.36
  217.9 9.9 %all-to-all-start.3 = ((bf16[32,24,128]{2,1,0:T(8,128)(2,1)}), bf16[32,24,128]{2,1,0:T(8,128)(2,1)S(1)}, u32[]{:S(2)}, u32[]{:S(2)}) async-start(bf16[32,24,128]{2,1,0:T(8,128)(2,1)} %bitcast.12), calls=%async_computation.3 | async-start | bytes 393216 | tf_op jit(solution)/shard_map/all_to_all | solution.py:111
  227.8 0.1 reduce_sum.51
  227.9 0.1 copy.32
  228.0 0.2 copy.33
  228.2 0.1 copy.28
  228.4 9.5 %all-to-all-done.3 = bf16[32,24,128]{2,1,0:T(8,128)(2,1)S(1)} async-done(((bf16[32,24,128]{2,1,0:T(8,128)(2,1)}), bf16[32,24,128]{2,1,0:T(8,128)(2,1)S(1)}, u32[]{:S(2)}, u32[]{:S(2)}) %all-to-all-start.3) | async-done | bytes 196640 | tf_op jit(solution)/shard_map/all_to_all | solution.py:111
  237.9 1.3 gather_fusion.1
  239.2 1.5 multiply_reduce_fusion
  240.7 1.5 add_convert_fusion
  (18 shorter events, 0.2 us)
Async XLA Ops:
  6.5 133.5 %copy-start = (bf16[1,264,2048]{2,1,0:T(8,128)(2,1)S(1)}, bf16[1,264,2048]{2,1,0:T(8,128)(2,1)}, u32[]{:S(2)}) copy-start(bf16[1,264,2048]{2,1,0:T(8,128)(2,1)} %param.25) | copy-start | bytes 3244036
  7.5 9.2 %collective-permute-start = (bf16[64,2]{1,0:T(8,128)(2,1)S(1)}, bf16[64,2]{1,0:T(8,128)(2,1)S(1)}, u32[]{:S(2)}, u32[]{:S(2)}) collective-permute-start(bf16[64,2]{1,0:T(8,128)(2,1)S(1)} %slice.52), channel_id=1, source_target_pairs={{0,16},{16,32},{32,48},{48,64},{64,80},{80,96},{96,112},{112,128},... | collective-permute-start | bytes 776 | tf_op jit(solution)/shard_map/ppermute | solution.py:12
  11.4 3.8 %collective-permute-start.1 = (s32[2]{0:T(128)S(1)}, s32[2]{0:T(128)S(1)}, u32[]{:S(2)}, u32[]{:S(2)}) collective-permute-start(s32[2]{0:T(128)S(1)} %slice.41), channel_id=1, source_target_pairs={{0,16},{16,32},{32,48},{48,64},{64,80},{80,96},{96,112},{112,128},... | collective-permute-start | bytes 32 | tf_op jit(solution)/shard_map/ppermute | solution.py:12
  18.3 10.0 %copy-start.1 = (s32[256,2]{0,1:T(2,128)S(1)}, s32[256,2]{0,1:T(2,128)}, u32[]{:S(2)}) copy-start(s32[256,2]{0,1:T(2,128)} %param.21) | copy-start | bytes 6148
  19.6 35.0 %all-to-all-start = ((bf16[16,256,128]{2,1,0:T(8,128)(2,1)}), bf16[16,256,128]{2,1,0:T(8,128)(2,1)S(1)}, u32[]{:S(2)}, u32[]{:S(2)}) async-start(bf16[16,256,128]{2,1,0:T(8,128)(2,1)} %bitcast.55), calls=%async_computation | async-start | bytes 2097152 | tf_op jit(solution)/shard_map/all_to_all | solution.py:22
  33.2 103.0 %copy-start.3 = (bf16[1,2048,264]{1,2,0:T(8,128)(2,1)S(1)}, bf16[1,2048,264]{1,2,0:T(8,128)(2,1)}, u32[]{:S(2)}) copy-start(bf16[1,2048,264]{1,2,0:T(8,128)(2,1)} %param.23) | copy-start | bytes 3244036
  56.3 9.7 %all-to-all-start.1 = ((f32[16,256,1]{1,2,0:T(1,128)}), f32[16,256,1]{1,2,0:T(1,128)S(1)}, u32[]{:S(2)}, u32[]{:S(2)}) async-start(f32[16,256,1]{1,2,0:T(1,128)} %broadcast_in_dim.67), calls=%async_computation.1 | async-start | bytes 32768 | tf_op jit(solution)/shard_map/all_to_all | solution.py:28
  61.5 74.6 %all-gather.2.cloned.1.call-start = ((), (), s32[]{:S(2)}) async-start(), calls=%async_computation.5 | async-start | bytes 3342336 | tf_op jit(solution)/shard_map/all_gather | solution.py:105
  94.2 45.8 %copy-start.4 = (bf16[1,2048,264]{1,2,0:T(8,128)(2,1)S(1)}, bf16[1,2048,264]{1,2,0:T(8,128)(2,1)}, u32[]{:S(2)}) copy-start(bf16[1,2048,264]{1,2,0:T(8,128)(2,1)} %param.24) | copy-start | bytes 3244036
  94.2 121.9 %reduce-scatter.4.cloned.1.call-start = ((), (), s32[]{:S(2)}) async-start(), calls=%async_computation.6 | async-start | bytes 3342336
  151.9 76.3 %copy-start.2 = (f32[256,2]{0,1:T(2,128)S(1)}, f32[256,2]{0,1:T(2,128)}, u32[]{:S(2)}) copy-start(f32[256,2]{0,1:T(2,128)} %param.22) | copy-start | bytes 6148
  217.9 20.0 %all-to-all-start.3 = ((bf16[32,24,128]{2,1,0:T(8,128)(2,1)}), bf16[32,24,128]{2,1,0:T(8,128)(2,1)S(1)}, u32[]{:S(2)}, u32[]{:S(2)}) async-start(bf16[32,24,128]{2,1,0:T(8,128)(2,1)} %bitcast.12), calls=%async_computation.3 | async-start | bytes 393216 | tf_op jit(solution)/shard_map/all_to_all | solution.py:111
Sparse Core Ops, SparseCore 0:
  94.3 41.7 all-gather.1
  152.1 63.9 reduce-scatter.3
where the time goes:
time: 250 us; the launch traced here: 249 us
  waiting for transfers between devices  138 us (55%)
  starting transfers between devices  30.1 us (12%)
  blocking collectives  25 us (10%)
  local copies, waits for them, and re-layouts  18.9 us (8%)
  between operations  13.7 us (5%)
  matrix products  12.7 us (5%)
  other arithmetic  10.6 us (4%)
    unnamed x3, waiting for transfers between devices  64.2 us
    all_gather x1, waiting for transfers between devices, shards(): piece_cols = lax.all_gather(row_block, 'tp', axis=1, tiled=True)  41.9 us
    all_to_all x1, blocking collectives, shards(): lax.all_to_all(picked, 'sp', split_axis=0, concat_axis=0, tiled=True)  25 us
    all_to_all x1, waiting for transfers between devices, sum_at_owner(): parts = lax.all_to_all(in_blocks(x, dim, count), axis, 0, 0, tiled=True)  21.4 us
    all_to_all x1, starting transfers between devices, shards(): lax.all_to_all(summed.reshape(experts, slot_count, share_width), 'sp', sp...  9.9 us
    all_to_all x1, waiting for transfers between devices, shards(): lax.all_to_all(summed.reshape(experts, slot_count, share_width), 'sp', sp...  9.55 us
    all_to_all x1, starting transfers between devices, sum_at_owner(): parts = lax.all_to_all(in_blocks(x, dim, count), axis, 0, 0, tiled=True)  8.75 us
    dot_general x1, matrix products, shards(): down_sum = jnp.dot(hidden, down_weight, preferred_element_type=jnp.float32)  7.29 us
  transfers between devices with their start and end apart: 7, of which 5 were waited for; matrix products, arithmetic and copies ran while one was open for 5% of the time, Pallas kernels for 0%

commit v1 on v0

v1 whole, which is shorter than its diff:
```python
import functools

import jax
import jax.numpy as jnp
from jax import lax
from jax.experimental import pallas as pl
from jax.experimental.pallas import tpu as pltpu
from jax.sharding import PartitionSpec as P

EPSILON = 1e-06
LANES = 128
BF16 = jnp.bfloat16
F32 = jnp.float32
MESH = pl.DeviceIdType.MESH


def dz_order(depth):
    return (0, 1, 3, 4, 5, 6, 2, 7) if depth == 8 else tuple(range(depth))


def layer_kernel(
    sizes,
    in_gate,
    out_gate,
    values,
    taps,
    docs,
    out_weight,
    gain,
    routes_t,
    weights_t,
    residual_hbm,
    gate_hbm,
    up_hbm,
    down_hbm,
    out_ref,
    gate_w,
    up_w,
    down_w,
    residual_cols,
    halo_gate,
    halo_values,
    halo_docs,
    mixed_all,
    proj_w,
    stream_ref,
    pick_ref,
    slot_cols,
    weight_cols,
    packed,
    rows_in,
    normed,
    hidden_ref,
    partial,
    send_right,
    send_left,
    recv_right,
    recv_left,
    result_out,
    result_in,
    local_sem,
    halo_send,
    halo_recv,
    proj_send,
    proj_recv,
    mixed_send,
    mixed_recv,
    mixed_core_send,
    mixed_core_recv,
    down_send,
    down_recv,
    scatter_send,
    scatter_recv,
    own_sem,
    gather_right_send,
    gather_right_recv,
    gather_left_send,
    gather_left_recv,
    gather_core_send,
    gather_core_recv,
    hidden_send,
    hidden_recv,
    reduce_right_send,
    reduce_right_recv,
    reduce_left_send,
    reduce_left_recv,
    return_send,
    return_recv,
    own_result_sem,
):
    nz, nx, ny, cap, chunks = sizes
    nsp, ntp = nz * nx, 2 * ny
    per_chunk = nsp // chunks
    rows = per_chunk * cap
    tokens = out_ref.shape[0]
    channels = in_gate.shape[0]
    model_width = ntp * LANES
    order = dz_order(nz)
    offsets = [(dz, dx) for dz in order for dx in range(nx)]

    sp = lax.axis_index("sp")
    tp = lax.axis_index("tp")
    z, x = sp // nx, sp % nx
    y, core = tp // 2, tp % 2
    other = 1 - core
    partner = y * 2 + other

    def at_sp(dz, dx):
        return ((z + dz + nz) % nz) * nx + (x + dx + nx) % nx

    def at_y(dy):
        return (y + dy + ny) % ny

    def remote(src, dst, send_sem, recv_sem, **where):
        return pltpu.make_async_remote_copy(
            src_ref=src,
            dst_ref=dst,
            send_sem=send_sem,
            recv_sem=recv_sem,
            device_id=where,
            device_id_type=MESH,
        )

    local = [
        pltpu.make_async_copy(
            residual_hbm.at[:, pl.ds(pl.multiple_of(tp * LANES, LANES), LANES)],
            residual_cols,
            local_sem.at[0],
        ),
        pltpu.make_async_copy(gate_hbm, gate_w, local_sem.at[1]),
        pltpu.make_async_copy(up_hbm, up_w, local_sem.at[2]),
    ]
    for j in range(ny):
        local.append(
            pltpu.make_async_copy(
                down_hbm.at[:, pl.ds(pl.multiple_of((2 * j + core) * LANES, LANES), LANES)],
                down_w.at[0, :, j * LANES : (j + 1) * LANES],
                local_sem.at[3 + j],
            )
        )
    for copy in local:
        copy.start()

    barrier = pltpu.get_barrier_semaphore()
    for d in range(1, nsp):
        pl.semaphore_signal(
            barrier, inc=1, device_id={"sp": (sp + d) % nsp}, device_id_type=MESH
        )
    for d in range(1, ntp):
        pl.semaphore_signal(
            barrier, inc=1, device_id={"tp": (tp + d) % ntp}, device_id_type=MESH
        )

    experts = lax.broadcasted_iota(jnp.int32, (nsp, tokens), 0)
    dz_of = (experts // nx - z + nz) % nz
    dx_of = (experts % nx - x + nx) % nx
    place = jnp.zeros_like(dz_of)
    for at, dz in enumerate(order):
        place = jnp.where(dz_of == dz, at, place)
    base = ((place * nx + dx_of) * cap).astype(F32)
    first = (experts == routes_t[0:1, :]).astype(F32)
    second = (experts == routes_t[1:2, :]).astype(F32)
    before = (
        lax.broadcasted_iota(jnp.int32, (tokens, tokens), 0)
        < lax.broadcasted_iota(jnp.int32, (tokens, tokens), 1)
    ).astype(F32)
    rank = jnp.dot(
        (first + second).astype(BF16), before.astype(BF16), preferred_element_type=F32
    )
    slots = base + rank
    slot_rows = [
        jnp.sum(first * slots, axis=0, keepdims=True),
        jnp.sum(second * slots, axis=0, keepdims=True),
    ]
    slot_at = lax.broadcasted_iota(jnp.int32, (nsp * cap, tokens), 0).astype(F32)
    pick_ref[...] = jnp.where(
        (slot_at == slot_rows[0]) | (slot_at == slot_rows[1]), 1.0, 0.0
    ).astype(BF16)
    diagonal = lax.broadcasted_iota(jnp.int32, (tokens, tokens), 0) == lax.broadcasted_iota(
        jnp.int32, (tokens, tokens), 1
    )
    for k in range(2):
        slot_cols[k] = jnp.sum(jnp.where(diagonal, slot_rows[k], 0.0), axis=1, keepdims=True)
        weight_cols[k] = jnp.sum(
            jnp.where(diagonal, weights_t[k : k + 1, :], 0.0), axis=1, keepdims=True
        )

    pl.semaphore_wait(barrier, nsp - 1 + ntp - 1)

    after = (sp + 1) % nsp
    last = slice(tokens - LANES, tokens)
    halo = [
        remote(in_gate.at[:, last], halo_gate, halo_send.at[0], halo_recv.at[0], sp=after),
        remote(values.at[:, last], halo_values, halo_send.at[1], halo_recv.at[1], sp=after),
        remote(docs.at[:, last], halo_docs, halo_send.at[2], halo_recv.at[2], sp=after),
    ]
    for copy in halo:
        copy.start()

    def weight_rows(owner):
        return pl.ds(pl.multiple_of(owner * channels, channels), channels)

    proj = []
    for d in range(1, ntp):
        to = (tp + d) % ntp
        copy = remote(
            out_weight.at[:, pl.ds(pl.multiple_of(to * LANES, LANES), LANES)],
            proj_w.at[weight_rows(tp)],
            proj_send.at[d],
            proj_recv.at[d],
            tp=to,
        )
        copy.start()
        proj.append(copy)
    proj_w[weight_rows(tp), :] = out_weight[:, pl.ds(pl.multiple_of(tp * LANES, LANES), LANES)]

    down = []
    for j in range(ny):
        copy = remote(
            down_hbm.at[:, pl.ds(pl.multiple_of((2 * j + other) * LANES, LANES), LANES)],
            down_w.at[1, :, j * LANES : (j + 1) * LANES],
            down_send.at[j],
            down_recv.at[j],
            tp=partner,
        )
        copy.start()
        down.append(copy)

    def shift(main, edge, by):
        wide = jnp.concatenate([edge] * (tokens // LANES), axis=1)
        lane = lax.broadcasted_iota(jnp.int32, main.shape, 1)
        return jnp.where(
            lane < by, pltpu.roll(wide, by, axis=1), pltpu.roll(main, by, axis=1)
        )

    gated = (in_gate[...].astype(F32) * values[...].astype(F32)).astype(BF16).astype(F32)
    doc_here = jnp.broadcast_to(docs[...].astype(F32), (8, tokens))
    channel_diagonal = lax.broadcasted_iota(
        jnp.int32, (channels, channels), 0
    ) == lax.broadcasted_iota(jnp.int32, (channels, channels), 1)
    tap = [
        jnp.sum(
            jnp.where(channel_diagonal, taps[i : i + 1, :].astype(F32), 0.0),
            axis=1,
            keepdims=True,
        )
        for i in range(3)
    ]
    for copy in halo:
        copy.wait_recv()
    edge = (halo_gate[...].astype(F32) * halo_values[...].astype(F32)).astype(BF16).astype(F32)
    doc_edge = jnp.broadcast_to(halo_docs[...].astype(F32), (8, LANES))
    doc_edge = jnp.where(sp == 0, -1.0, doc_edge)
    near = (shift(doc_here, doc_edge, 1) == doc_here).astype(F32)[0:1, :]
    far = (shift(doc_here, doc_edge, 2) == doc_here).astype(F32)[0:1, :]
    convolved = (
        tap[2] * gated + tap[1] * shift(gated, edge, 1) * near + tap[0] * shift(gated, edge, 2) * far
    )
    mixed_all[weight_rows(tp), :] = (out_gate[...].astype(F32) * convolved).astype(BF16)

    mixed = []
    own_mixed = mixed_all.at[weight_rows(tp)]
    for d in range(1, ny):
        copy = remote(
            own_mixed,
            own_mixed,
            mixed_send.at[d],
            mixed_recv.at[d],
            tp=at_y(d) * 2 + core,
        )
        copy.start()
        mixed.append(copy)
    mixed_core = []
    for d in range(ny):
        from_chip = at_y(-d)
        arrived = mixed_all.at[weight_rows(from_chip * 2 + core)]
        if d:
            remote(
                arrived, arrived, mixed_send.at[d], mixed_recv.at[d], tp=from_chip * 2 + core
            ).wait_recv()
        copy = remote(
            arrived, arrived, mixed_core_send.at[d], mixed_core_recv.at[d], tp=partner
        )
        copy.start()
        mixed_core.append(copy)
    for copy in proj:
        copy.wait_recv()
    local[0].wait()
    for d in range(ny):
        arrived = mixed_all.at[weight_rows(at_y(-d) * 2 + other)]
        remote(
            arrived, arrived, mixed_core_send.at[d], mixed_core_recv.at[d], tp=partner
        ).wait_recv()
    projected = lax.dot_general(
        mixed_all[...], proj_w[...], (((0,), (0,)), ((), ())), preferred_element_type=F32
    )
    stream = residual_cols[...].astype(F32) + projected
    stream_ref[...] = stream

    packed[...] = (
        jnp.dot(pick_ref[...], stream.astype(BF16), preferred_element_type=F32)
        .reshape(nsp, cap, LANES)
        .astype(BF16)
    )

    def scatter(o):
        dz, dx = offsets[o]
        c, g = divmod(o, per_chunk)
        return remote(
            packed.at[o],
            rows_in.at[c, tp, g],
            scatter_send.at[o],
            scatter_recv.at[o],
            sp=at_sp(dz, dx),
        )

    own_rows = pltpu.make_async_copy(packed.at[0], rows_in.at[0, tp, 0], own_sem)
    own_rows.start()
    for o in range(1, nsp):
        scatter(o).start()

    def reach(c):
        long, short = ny // 2, ny - 1 - ny // 2
        return (long, short) if c % 2 == 0 else (short, long)

    def block(c, chip, of_core):
        return rows_in.at[c, chip * 2 + of_core]

    def gather_right(c, h):
        ref = block(c, at_y(-h), core)
        return remote(
            ref,
            ref,
            gather_right_send.at[c, h],
            gather_right_recv.at[c, h],
            tp=at_y(1) * 2 + core,
        )

    def gather_left(c, h):
        ref = block(c, at_y(h), core)
        return remote(
            ref, ref, gather_left_send.at[c, h], gather_left_recv.at[c, h], tp=at_y(-1) * 2 + core
        )

    def arrived_right(c, h):
        ref = block(c, at_y(-h), core)
        return remote(
            ref,
            ref,
            gather_right_send.at[c, h - 1],
            gather_right_recv.at[c, h - 1],
            tp=at_y(1) * 2 + core,
        )

    def arrived_left(c, h):
        ref = block(c, at_y(h), core)
        return remote(
            ref,
            ref,
            gather_left_send.at[c, h - 1],
            gather_left_recv.at[c, h - 1],
            tp=at_y(-1) * 2 + core,
        )

    def core_index(c, dy):
        right, left = reach(c)
        return -dy if dy <= 0 else right + dy

    def gather_core(c, dy, of_core):
        ref = block(c, at_y(dy), of_core)
        j = core_index(c, dy)
        return remote(
            ref, ref, gather_core_send.at[c, j], gather_core_recv.at[c, j], tp=partner
        )

    def gather_start(c):
        for g in range(per_chunk):
            o = c * per_chunk + g
            if o == 0:
                own_rows.wait()
            else:
                remote(
                    packed.at[o],
                    rows_in.at[c, tp, g],
                    scatter_send.at[o],
                    scatter_recv.at[o],
                    sp=at_sp(0, 0),
                ).wait_recv()
        right, left = reach(c)
        if right:
            gather_right(c, 0).start()
        if left:
            gather_left(c, 0).start()
        gather_core(c, 0, core).start()

    def gather_hop(c, h):
        right, left = reach(c)
        if h <= right:
            arrived_right(c, h).wait_recv()
            if h < right:
                gather_right(c, h).start()
            gather_core(c, -h, core).start()
        if h <= left:
            arrived_left(c, h).wait_recv()
            if h < left:
                gather_left(c, h).start()
            gather_core(c, h, core).start()

    def gate_up(c):
        right, left = reach(c)
        for dy in range(-right, left + 1):
            gather_core(c, dy, other).wait_recv()
        if c == 0:
            local[1].wait()
            local[2].wait()
        squares = jnp.zeros((rows, LANES), F32)
        for b in range(ntp):
            part = rows_in[c, b].astype(F32).reshape(rows, LANES)
            squares = squares + part * part
        inverse = lax.rsqrt(
            jnp.sum(squares, axis=1, keepdims=True) / model_width + EPSILON
        )
        for b in range(ntp):
            at = slice(b * LANES, (b + 1) * LANES)
            part = rows_in[c, b].astype(F32).reshape(rows, LANES)
            normed[:, at] = (part * inverse * gain[:, at].astype(F32)).astype(BF16)
        contract = (((1,), (1,)), ((), ()))
        gate_sum = lax.dot_general(normed[...], gate_w[...], contract, preferred_element_type=F32)
        up_sum = lax.dot_general(normed[...], up_w[...], contract, preferred_element_type=F32)
        hidden_ref[c, 0] = (gate_sum / (1.0 + jnp.exp(-gate_sum)) * up_sum).astype(BF16)
        hidden_copy(c).start()

    def hidden_copy(c):
        return remote(
            hidden_ref.at[c, 0], hidden_ref.at[c, 1], hidden_send.at[c], hidden_recv.at[c], tp=partner
        )

    def down_sum(c):
        if c == 0:
            for copy in local[3:]:
                copy.wait()
            for copy in down:
                copy.wait_recv()
        hidden_copy(c).wait_recv()
        total = jnp.dot(hidden_ref[c, 0], down_w[0], preferred_element_type=F32) + jnp.dot(
            hidden_ref[c, 1], down_w[1], preferred_element_type=F32
        )
        for j in range(ny):
            partial[c, j] = total[:, j * LANES : (j + 1) * LANES]

    def reduce_right(c, s):
        return remote(
            send_right.at[c, s],
            recv_right.at[c, s],
            reduce_right_send.at[c, s],
            reduce_right_recv.at[c, s],
            tp=at_y(1) * 2 + core,
        )

    def reduce_left(c, s):
        return remote(
            send_left.at[c, s],
            recv_left.at[c, s],
            reduce_left_send.at[c, s],
            reduce_left_recv.at[c, s],
            tp=at_y(-1) * 2 + core,
        )

    def reduce_step(c, s):
        right, left = reach(c)
        if s < right:
            share = partial[c, at_y(right - s)]
            if s:
                reduce_right(c, s - 1).wait_recv()
                share = share + recv_right[c, s - 1].astype(F32)
            send_right[c, s] = share.astype(BF16)
            reduce_right(c, s).start()
        if s < left:
            share = partial[c, at_y(s - left)]
            if s:
                reduce_left(c, s - 1).wait_recv()
                share = share + recv_left[c, s - 1].astype(F32)
            send_left[c, s] = share.astype(BF16)
            reduce_left(c, s).start()

    def give_back(o):
        dz, dx = offsets[o]
        c, g = divmod(o, per_chunk)
        return remote(
            result_out.at[c, g],
            result_in.at[o],
            return_send.at[o],
            return_recv.at[o],
            sp=at_sp(-dz, -dx),
        )

    own_result = pltpu.make_async_copy(result_out.at[0, 0], result_in.at[0], own_result_sem)

    def reduce_last(c):
        right, left = reach(c)
        total = partial[c, y]
        if right:
            reduce_right(c, right - 1).wait_recv()
            total = total + recv_right[c, right - 1].astype(F32)
        if left:
            reduce_left(c, left - 1).wait_recv()
            total = total + recv_left[c, left - 1].astype(F32)
        result_out[c] = total.reshape(per_chunk, cap, LANES).astype(BF16)
        for g in range(per_chunk):
            if c == 0 and g == 0:
                own_result.start()
            else:
                give_back(c * per_chunk + g).start()

    hops = ny // 2
    for wave in range(chunks + 2 * hops):
        for c in range(chunks):
            h = wave - c
            if h == 0:
                gather_start(c)
            elif 1 <= h <= hops:
                gather_hop(c, h)
        for c in range(chunks):
            s = wave - c - hops
            if 1 <= s < hops:
                reduce_step(c, s)
            elif s == hops:
                reduce_last(c)
        for c in range(chunks):
            if wave - c == hops:
                gate_up(c)
                down_sum(c)
                reduce_step(c, 0)

    blended = [jnp.zeros((tokens, LANES), F32), jnp.zeros((tokens, LANES), F32)]
    for c in range(chunks):
        for g in range(per_chunk):
            o = c * per_chunk + g
            if o == 0:
                own_result.wait()
            else:
                give_back(o).wait_recv()
        result = (
            result_in[c * per_chunk : (c + 1) * per_chunk]
            .astype(F32)
            .reshape(rows, LANES)
            .astype(BF16)
        )
        at = lax.broadcasted_iota(jnp.int32, (tokens, rows), 1) + c * rows
        for k in range(2):
            choose = jnp.where(at.astype(F32) == slot_cols[k], 1.0, 0.0).astype(BF16)
            blended[k] = blended[k] + jnp.dot(choose, result, preferred_element_type=F32)
    out_ref[...] = (
        stream_ref[...] + weight_cols[0] * blended[0] + weight_cols[1] * blended[1]
    ).astype(out_ref.dtype)

    for copy in halo + proj + down + mixed + mixed_core:
        copy.wait_send()
    for o in range(1, nsp):
        scatter(o).wait_send()
        give_back(o).wait_send()
    for c in range(chunks):
        right, left = reach(c)
        for h in range(right):
            gather_right(c, h).wait_send()
            reduce_right(c, h).wait_send()
        for h in range(left):
            gather_left(c, h).wait_send()
            reduce_left(c, h).wait_send()
        for dy in range(-right, left + 1):
            gather_core(c, dy, core).wait_send()
        hidden_copy(c).wait_send()


def layer(
    sizes,
    in_gate,
    out_gate,
    values,
    conv_taps,
    doc_ids,
    residual,
    out_weight,
    norm_gain,
    routes,
    route_weights,
    expert_gate,
    expert_up,
    expert_down,
):
    nz, nx, ny, cap, chunks = sizes
    nsp, ntp = nz * nx, 2 * ny
    per_chunk = nsp // chunks
    rows = per_chunk * cap
    tokens = doc_ids.shape[0]
    channels = in_gate.shape[0]
    units = expert_down.shape[1]
    hops = ny // 2
    vmem = pl.BlockSpec(memory_space=pltpu.VMEM)
    hbm = pl.BlockSpec(memory_space=pl.ANY)
    dma = pltpu.SemaphoreType.DMA
    return pl.pallas_call(
        functools.partial(layer_kernel, sizes),
        out_shape=jax.ShapeDtypeStruct((tokens, LANES), BF16),
        in_specs=[vmem] * 9 + [hbm] * 4,
        out_specs=vmem,
        scratch_shapes=[
            pltpu.VMEM((units, ntp * LANES), BF16),
            pltpu.VMEM((units, ntp * LANES), BF16),
            pltpu.VMEM((2, units, ny * LANES), BF16),
            pltpu.VMEM((tokens, LANES), BF16),
            pltpu.VMEM((channels, LANES), BF16),
            pltpu.VMEM((channels, LANES), BF16),
            pltpu.VMEM((1, LANES), jnp.int32),
            pltpu.VMEM((ntp * channels, tokens), BF16),
            pltpu.VMEM((ntp * channels, LANES), BF16),
            pltpu.VMEM((tokens, LANES), F32),
            pltpu.VMEM((nsp * cap, tokens), BF16),
            pltpu.VMEM((2, tokens, 1), F32),
            pltpu.VMEM((2, tokens, 1), F32),
            pltpu.VMEM((nsp, cap, LANES), BF16),
            pltpu.VMEM((chunks, ntp, per_chunk, cap, LANES), BF16),
            pltpu.VMEM((rows, ntp * LANES), BF16),
            pltpu.VMEM((chunks, 2, rows, units), BF16),
            pltpu.VMEM((chunks, ny, rows, LANES), F32),
            pltpu.VMEM((chunks, hops, rows, LANES), BF16),
            pltpu.VMEM((chunks, hops, rows, LANES), BF16),
            pltpu.VMEM((chunks, hops, rows, LANES), BF16),
            pltpu.VMEM((chunks, hops, rows, LANES), BF16),
            pltpu.VMEM((chunks, per_chunk, cap, LANES), BF16),
            pltpu.VMEM((nsp, cap, LANES), BF16),
            dma((3 + ny,)),
            dma((3,)),
            dma((3,)),
            dma((ntp,)),
            dma((ntp,)),
            dma((ny,)),
            dma((ny,)),
            dma((ny,)),
            dma((ny,)),
            dma((ny,)),
            dma((ny,)),
            dma((nsp,)),
            dma((nsp,)),
            dma,
            dma((chunks, hops)),
            dma((chunks, hops)),
            dma((chunks, hops)),
            dma((chunks, hops)),
            dma((chunks, ny)),
            dma((chunks, ny)),
            dma((chunks,)),
            dma((chunks,)),
            dma((chunks, hops)),
            dma((chunks, hops)),
            dma((chunks, hops)),
            dma((chunks, hops)),
            dma((nsp,)),
            dma((nsp,)),
            dma,
        ],
        compiler_params=pltpu.CompilerParams(
            collective_id=0, has_side_effects=True, vmem_limit_bytes=60 * 1024 * 1024
        ),
        name="layer",
    )(
        in_gate,
        out_gate,
        values,
        conv_taps,
        doc_ids.reshape(1, tokens),
        out_weight,
        norm_gain.reshape(1, -1),
        routes.T,
        route_weights.T,
        residual,
        jnp.swapaxes(expert_gate, 1, 2)[0],
        jnp.swapaxes(expert_up, 1, 2)[0],
        expert_down[0],
    )


def solution(mesh):
    placed = (
        P("tp", "sp"),
        P("tp", "sp"),
        P("tp", "sp"),
        P(None, "tp"),
        P("sp"),
        P("sp", None),
        P("tp", None),
        P(),
        P("sp", None),
        P("sp", None),
        P("sp", None, "tp"),
        P("sp", None, "tp"),
        P("sp", "tp", None),
    )
    sizes = (mesh.shape["sp"] // 4, 4, mesh.shape["tp"] // 2, 24, 4)
    return jax.shard_map(
        functools.partial(layer, sizes),
        mesh=mesh,
        in_specs=placed,
        out_specs=P("sp", "tp"),
        check_vma=False,
    )
```

time: 250 us -> 103 us (0.41)
  the two profiles are of different devices: /device:TPU:25 before, /device:TPU:8 now
where the time goes in v1:
time: 103 us
  Pallas kernels  99.9 us (97%)
  local copies, waits for them, and re-layouts  2.76 us (3%)
    pallas_call x1, Pallas kernels, layer(): pl.pallas_call(functools.partial(layer_kernel, sizes), out_shape=jax.Shap...  99.9 us

profile of v1, /device:TPU:8, one launch (start us, length us, event | category | flops | bytes accessed | tf_op | source)
XLA Modules:
  0.0 102.7 jit_solution(13362790452376071160)
XLA Ops:
  0.0 1.3 %reshape.7.gain = bf16[1,2048]{1,0:T(2,128)(2,1)} reshape(bf16[2048]{0:T(1024)(128)(2,1)} %param.20) | data formatting | bytes 8192 | tf_op jit(solution)/shard_map/reshape | solution.py:673
  1.3 99.9 %layer.1 = bf16[256,128]{1,0:T(8,128)(2,1)} custom-call(bf16[64,256]{1,0:T(8,128)(2,1)} %in_gate.1, bf16[64,256]{1,0:T(8,128)(2,1)} %out_gate.1, bf16[64,256]{1,0:T(8,128)(2,1)} %values.1, bf16[3,64]{1,0:T(4,128)(2,1)} %taps.1, s32[1,256]{1,0:T(1,128)} %bitcast.15, bf16[64,2048]{1,0:T(8,128)(2,1)} %out_weight.1, bf16[1,2048]{1,0:T(2,128)(2,1)} %reshape.7.gain, ...), custom_call_target="tpu_custom_call" | custom-call | tf_op jit(solution)/shard_map/layer/pallas_call | solution.py:602
  101.2 1.5 %copy.15 = bf16[256,128]{1,0:T(8,128)(2,1)} copy(bf16[256,128]{1,0:T(8,128)(2,1)} %layer.1) | data formatting | bytes 131072

commit v2 on v1

v2 whole, which is shorter than its diff:
```python
import functools

import jax
import jax.numpy as jnp
from jax import lax
from jax.experimental import pallas as pl
from jax.experimental.pallas import tpu as pltpu
from jax.sharding import PartitionSpec as P

EPSILON = 1e-06
LANES = 128
BF16 = jnp.bfloat16
F32 = jnp.float32
MESH = pl.DeviceIdType.MESH


def dz_order(depth):
    return (1, 6, 3, 5, 4, 2, 0, 7) if depth == 8 else tuple(range(depth))[::-1]


def schedule(chunks, hops):
    steps = [("start", c) for c in range(chunks)]
    for h in range(1, hops):
        steps += [("hop", c, h) for c in range(chunks)]
    early = chunks // 2
    for c in range(chunks + 2):
        if c < chunks:
            steps += [("hop", c, hops)]
        if 0 <= c - 1 < chunks:
            steps += [("gate", c - 1)]
        if 0 <= c - 2 < chunks:
            steps += [("down", c - 2), ("add", c - 2, 0)]
            if c - 2 >= early:
                steps += [("add", c - 2 - early, 1)]
    for s in range(1, hops):
        steps += [("add", c, s) for c in range(chunks) if s > 1 or c >= chunks - early]
    return steps + [("last", c) for c in range(chunks)]


def layer_kernel(
    sizes,
    in_gate_hbm,
    out_gate_hbm,
    values_hbm,
    taps_hbm,
    docs_hbm,
    out_weight_hbm,
    gain_hbm,
    routes_hbm,
    weights_hbm,
    residual_hbm,
    gate_hbm,
    up_hbm,
    down_hbm,
    out_ref,
    in_gate,
    out_gate,
    values,
    taps,
    docs,
    out_weight,
    gain,
    routes_t,
    weights_t,
    gate_w,
    up_w,
    down_w,
    residual_cols,
    halo_gate,
    halo_values,
    halo_docs,
    mixed_all,
    proj_w,
    edge_out,
    edge_in,
    stream_ref,
    pick_ref,
    slot_cols,
    weight_cols,
    packed,
    rows_in,
    normed,
    hidden_ref,
    partial,
    send_right,
    send_left,
    recv_right,
    recv_left,
    result_out,
    result_in,
    local_sem,
    halo_send,
    halo_recv,
    proj_send,
    proj_recv,
    edge_send,
    edge_recv,
    mixed_right_send,
    mixed_right_recv,
    mixed_left_send,
    mixed_left_recv,
    mixed_core_send,
    mixed_core_recv,
    down_send,
    down_recv,
    scatter_send,
    scatter_recv,
    own_sem,
    gather_right_send,
    gather_right_recv,
    gather_left_send,
    gather_left_recv,
    gather_core_send,
    gather_core_recv,
    hidden_send,
    hidden_recv,
    reduce_right_send,
    reduce_right_recv,
    reduce_left_send,
    reduce_left_recv,
    return_send,
    return_recv,
    own_result_sem,
):
    nz, nx, ny, cap, chunks = sizes
    nsp, ntp = nz * nx, 2 * ny
    per_chunk = nsp // chunks
    rows = per_chunk * cap
    tokens = out_ref.shape[0]
    channels = in_gate.shape[0]
    model_width = ntp * LANES
    order = dz_order(nz)
    offsets = [(dz, dx) for dz in order for dx in range(nx)]
    others = [o for o in range(nsp) if offsets[o] != (0, 0)]
    own = offsets.index((0, 0))
    own_chunk = own // per_chunk
    assert own % per_chunk == 0

    sp = lax.axis_index("sp")
    tp = lax.axis_index("tp")
    z, x = sp // nx, sp % nx
    y, core = tp // 2, tp % 2
    other = 1 - core
    partner = y * 2 + other

    def at_sp(dz, dx):
        return ((z + dz + nz) % nz) * nx + (x + dx + nx) % nx

    def at_y(dy):
        return (y + dy + ny) % ny

    def remote(src, dst, send_sem, recv_sem, **where):
        return pltpu.make_async_remote_copy(
            src_ref=src,
            dst_ref=dst,
            send_sem=send_sem,
            recv_sem=recv_sem,
            device_id=where,
            device_id_type=MESH,
        )

    def all_of(ref, sem):
        pltpu.make_async_copy(ref, ref, sem).wait()

    barrier = pltpu.get_barrier_semaphore()
    for d in range(1, nsp):
        pl.semaphore_signal(
            barrier, inc=1, device_id={"sp": (sp + d) % nsp}, device_id_type=MESH
        )
    for d in range(1, ntp):
        pl.semaphore_signal(
            barrier, inc=1, device_id={"tp": (tp + d) % ntp}, device_id_type=MESH
        )

    staged = [
        (routes_hbm, routes_t),
        (weights_hbm, weights_t),
        (in_gate_hbm, in_gate),
        (values_hbm, values),
        (docs_hbm, docs),
        (out_weight_hbm, out_weight),
        (out_gate_hbm, out_gate),
        (taps_hbm, taps),
        (residual_hbm.at[:, pl.ds(pl.multiple_of(tp * LANES, LANES), LANES)], residual_cols),
        (gain_hbm, gain),
        (gate_hbm, gate_w),
        (up_hbm, up_w),
    ]
    staged = [
        pltpu.make_async_copy(src, dst, local_sem.at[i]) for i, (src, dst) in enumerate(staged)
    ]
    down_own = [
        pltpu.make_async_copy(
            down_hbm.at[:, pl.ds(pl.multiple_of((2 * j + core) * LANES, LANES), LANES)],
            down_w.at[0, :, j * LANES : (j + 1) * LANES],
            local_sem.at[len(staged)],
        )
        for j in range(ny)
    ]
    for copy in staged + down_own:
        copy.start()
    for copy in staged[:2]:
        copy.wait()

    experts = lax.broadcasted_iota(jnp.int32, (nsp, tokens), 0)
    dz_of = (experts // nx - z + nz) % nz
    dx_of = (experts % nx - x + nx) % nx
    place = jnp.zeros_like(dz_of)
    for at, dz in enumerate(order):
        place = jnp.where(dz_of == dz, at, place)
    base = ((place * nx + dx_of) * cap).astype(F32)
    first = (experts == routes_t[0:1, :]).astype(F32)
    second = (experts == routes_t[1:2, :]).astype(F32)
    before = (
        lax.broadcasted_iota(jnp.int32, (tokens, tokens), 0)
        < lax.broadcasted_iota(jnp.int32, (tokens, tokens), 1)
    ).astype(F32)
    rank = jnp.dot(
        (first + second).astype(BF16), before.astype(BF16), preferred_element_type=F32
    )
    slots = base + rank
    slot_rows = [
        jnp.sum(first * slots, axis=0, keepdims=True),
        jnp.sum(second * slots, axis=0, keepdims=True),
    ]
    slot_at = lax.broadcasted_iota(jnp.int32, (nsp * cap, tokens), 0).astype(F32)
    pick_ref[...] = jnp.where(
        (slot_at == slot_rows[0]) | (slot_at == slot_rows[1]), 1.0, 0.0
    ).astype(BF16)
    diagonal = lax.broadcasted_iota(jnp.int32, (tokens, tokens), 0) == lax.broadcasted_iota(
        jnp.int32, (tokens, tokens), 1
    )
    for k in range(2):
        slot_cols[k] = jnp.sum(jnp.where(diagonal, slot_rows[k], 0.0), axis=1, keepdims=True)
        weight_cols[k] = jnp.sum(
            jnp.where(diagonal, weights_t[k : k + 1, :], 0.0), axis=1, keepdims=True
        )

    def weight_rows(owner):
        return pl.ds(pl.multiple_of(owner * channels, channels), channels)

    def convolve(here, doc, shifted, out):
        near = (shifted[1][1] == doc).astype(F32)[0:1, :]
        far = (shifted[2][1] == doc).astype(F32)[0:1, :]
        convolved = (
            tap[2] * here + tap[1] * shifted[1][0] * near + tap[0] * shifted[2][0] * far
        )
        return out.astype(F32) * convolved

    for copy in staged[2:8]:
        copy.wait()
    gated = (in_gate[...].astype(F32) * values[...].astype(F32)).astype(BF16).astype(F32)
    doc_here = jnp.broadcast_to(docs[...].astype(F32), (8, tokens))
    channel_diagonal = lax.broadcasted_iota(
        jnp.int32, (channels, channels), 0
    ) == lax.broadcasted_iota(jnp.int32, (channels, channels), 1)
    tap = [
        jnp.sum(
            jnp.where(channel_diagonal, taps[i : i + 1, :].astype(F32), 0.0),
            axis=1,
            keepdims=True,
        )
        for i in range(3)
    ]
    rolled = {
        by: (pltpu.roll(gated, by, axis=1), pltpu.roll(doc_here, by, axis=1)) for by in (1, 2)
    }
    lane = lax.broadcasted_iota(jnp.int32, (channels, tokens), 1)
    mixed_all[weight_rows(tp), :] = jnp.where(
        lane < 2, 0.0, convolve(gated, doc_here, rolled, out_gate[...])
    ).astype(BF16)
    proj_w[weight_rows(tp), :] = out_weight[:, pl.ds(pl.multiple_of(tp * LANES, LANES), LANES)]

    pl.semaphore_wait(barrier, nsp - 1 + ntp - 1)

    after = (sp + 1) % nsp
    last = slice(tokens - LANES, tokens)
    halo = [
        remote(in_gate.at[:, last], halo_gate, halo_send.at[0], halo_recv.at[0], sp=after),
        remote(values.at[:, last], halo_values, halo_send.at[1], halo_recv.at[1], sp=after),
        remote(docs.at[:, last], halo_docs, halo_send.at[2], halo_recv.at[2], sp=after),
    ]
    for copy in halo:
        copy.start()

    mixed_reach = (ny // 2, ny - 1 - ny // 2)

    def mixed_right(h):
        ref = mixed_all.at[weight_rows(at_y(-h) * 2 + core)]
        at = mixed_right_recv.at[h]
        return remote(ref, ref, mixed_right_send, at, tp=at_y(1) * 2 + core)

    def mixed_left(h):
        ref = mixed_all.at[weight_rows(at_y(h) * 2 + core)]
        at = mixed_left_recv.at[h]
        return remote(ref, ref, mixed_left_send, at, tp=at_y(-1) * 2 + core)

    def mixed_core(dy):
        ref = mixed_all.at[weight_rows(at_y(dy) * 2 + core)]
        return remote(ref, ref, mixed_core_send, mixed_core_recv, tp=partner)

    def mixed_arrived(dy, sem):
        all_of(mixed_all.at[weight_rows(at_y(dy) * 2 + core)], sem)

    def proj(to):
        return remote(
            out_weight.at[:, pl.ds(pl.multiple_of(to * LANES, LANES), LANES)],
            proj_w.at[weight_rows(tp)],
            proj_send,
            proj_recv,
            tp=to,
        )

    def mixed_hop(h):
        right, left = mixed_reach
        if h <= right:
            if h:
                mixed_arrived(-h, mixed_right_recv.at[h - 1])
            if h < right:
                mixed_right(h).start()
        if h <= left:
            if h:
                mixed_arrived(h, mixed_left_recv.at[h - 1])
            if h < left:
                mixed_left(h).start()
        if h <= right:
            mixed_core(-h).start()
        if h and h <= left:
            mixed_core(h).start()

    def edge(to):
        return remote(edge_out.at[to], edge_in.at[tp], edge_send, edge_recv, tp=to)

    def edge_rows():
        for copy in halo:
            copy.wait_recv()
        before_edge = (
            (halo_gate[...].astype(F32) * halo_values[...].astype(F32)).astype(BF16).astype(F32)
        )
        doc_edge = jnp.broadcast_to(halo_docs[...].astype(F32), (8, LANES))
        doc_edge = jnp.where(sp == 0, -1.0, doc_edge)
        first_gated, first_docs = gated[:, :LANES], doc_here[:, :LANES]

        def shift(main, edge, by):
            at = lax.broadcasted_iota(jnp.int32, main.shape, 1)
            return jnp.where(
                at < by, pltpu.roll(edge, by, axis=1), pltpu.roll(main, by, axis=1)
            )

        shifted = {
            by: (shift(first_gated, before_edge, by), shift(first_docs, doc_edge, by))
            for by in (1, 2)
        }
        mixed_edge = jnp.where(
            lane[:, :LANES] < 2,
            convolve(first_gated, first_docs, shifted, out_gate[:, :LANES]),
            0.0,
        )
        share = jnp.dot(
            mixed_edge.T[:16, :].astype(BF16), out_weight[...], preferred_element_type=F32
        )
        for j in range(ntp):
            edge_out[j] = share[:8, j * LANES : (j + 1) * LANES]
        for d in range(1, ntp):
            edge((tp + d) % ntp).start()
        edge_in[tp] = edge_out[tp]

    distances = sorted(range(1, ny), key=lambda d: -min(d, ny - d))
    batches = [distances[i : i + 2] for i in range(0, len(distances), 2)]
    for h in range(max(mixed_reach) + 1):
        mixed_hop(h)
        if h == 0:
            proj(partner).start()
        if h < len(batches):
            for d in batches[h]:
                proj(at_y(d) * 2 + core).start()
                proj(at_y(d) * 2 + other).start()
        if h == min(2, max(mixed_reach)):
            edge_rows()
    for h in range(max(mixed_reach) + 1, len(batches)):
        for d in batches[h]:
            proj(at_y(d) * 2 + core).start()
            proj(at_y(d) * 2 + other).start()
    all_of(proj_w.at[: (ntp - 1) * channels], proj_recv)
    staged[8].wait()
    all_of(mixed_all.at[: ny * channels], mixed_core_recv)
    projected = lax.dot_general(
        mixed_all[...], proj_w[...], (((0,), (0,)), ((), ())), preferred_element_type=F32
    )
    stream_ref[...] = residual_cols[...].astype(F32) + projected
    all_of(edge_in.at[: ntp - 1], edge_recv)
    stream_ref[:8, :] = stream_ref[:8, :] + jnp.sum(edge_in[...], axis=0)
    stream = stream_ref[...]

    packed[...] = (
        jnp.dot(pick_ref[...], stream.astype(BF16), preferred_element_type=F32)
        .reshape(nsp, cap, LANES)
        .astype(BF16)
    )

    def scatter(o):
        dz, dx = offsets[o]
        c, g = divmod(o, per_chunk)
        return remote(
            packed.at[o],
            rows_in.at[c, tp, g],
            scatter_send,
            scatter_recv.at[c],
            sp=at_sp(dz, dx),
        )

    own_rows = pltpu.make_async_copy(packed.at[own], rows_in.at[own_chunk, tp, 0], own_sem)
    own_rows.start()
    for o in others:
        scatter(o).start()

    for j in range(ny):
        remote(
            down_hbm.at[:, pl.ds(pl.multiple_of((2 * j + other) * LANES, LANES), LANES)],
            down_w.at[1, :, j * LANES : (j + 1) * LANES],
            down_send,
            down_recv,
            tp=partner,
        ).start()

    def reach(c):
        long, short = ny // 2, ny - 1 - ny // 2
        return (long, short) if c % 2 == 0 else (short, long)

    def block(c, chip, of_core):
        return rows_in.at[c, chip * 2 + of_core]

    def gather_right(c, h):
        ref = block(c, at_y(-h), core)
        return remote(
            ref,
            ref,
            gather_right_send,
            gather_right_recv.at[c, h],
            tp=at_y(1) * 2 + core,
        )

    def gather_left(c, h):
        ref = block(c, at_y(h), core)
        return remote(
            ref, ref, gather_left_send, gather_left_recv.at[c, h], tp=at_y(-1) * 2 + core
        )

    def arrived_right(c, h):
        ref = block(c, at_y(-h), core)
        return remote(
            ref,
            ref,
            gather_right_send,
            gather_right_recv.at[c, h - 1],
            tp=at_y(1) * 2 + core,
        )

    def arrived_left(c, h):
        ref = block(c, at_y(h), core)
        return remote(
            ref,
            ref,
            gather_left_send,
            gather_left_recv.at[c, h - 1],
            tp=at_y(-1) * 2 + core,
        )

    def gather_core(c, dy):
        ref = block(c, at_y(dy), core)
        return remote(ref, ref, gather_core_send, gather_core_recv.at[c], tp=partner)

    def gather_start(c):
        if c == own_chunk:
            own_rows.wait()
        alone = 1 if c == own_chunk else 0
        if alone < per_chunk:
            all_of(rows_in.at[c, tp, alone:], scatter_recv.at[c])
        right, left = reach(c)
        if right:
            gather_right(c, 0).start()
        if left:
            gather_left(c, 0).start()
        gather_core(c, 0).start()

    def gather_hop(c, h):
        right, left = reach(c)
        if h <= right:
            arrived_right(c, h).wait_recv()
            if h < right:
                gather_right(c, h).start()
            gather_core(c, -h).start()
        if h <= left:
            arrived_left(c, h).wait_recv()
            if h < left:
                gather_left(c, h).start()
            gather_core(c, h).start()

    def gate_up(c):
        all_of(rows_in.at[c, :ny], gather_core_recv.at[c])
        if c == 0:
            for copy in staged[9:]:
                copy.wait()
        squares = jnp.zeros((rows, LANES), F32)
        for b in range(ntp):
            part = rows_in[c, b].astype(F32).reshape(rows, LANES)
            squares = squares + part * part
        inverse = lax.rsqrt(
            jnp.sum(squares, axis=1, keepdims=True) / model_width + EPSILON
        )
        for b in range(ntp):
            at = slice(b * LANES, (b + 1) * LANES)
            part = rows_in[c, b].astype(F32).reshape(rows, LANES)
            normed[:, at] = (part * inverse * gain[b : b + 1, :].astype(F32)).astype(BF16)
        contract = (((1,), (1,)), ((), ()))
        gate_sum = lax.dot_general(normed[...], gate_w[...], contract, preferred_element_type=F32)
        up_sum = lax.dot_general(normed[...], up_w[...], contract, preferred_element_type=F32)
        hidden_ref[c, 0] = (gate_sum / (1.0 + jnp.exp(-gate_sum)) * up_sum).astype(BF16)
        hidden_copy(c).start()

    def hidden_copy(c):
        return remote(
            hidden_ref.at[c, 0], hidden_ref.at[c, 1], hidden_send, hidden_recv.at[c], tp=partner
        )

    def down_sum(c):
        if c == 0:
            all_of(down_w.at[0], local_sem.at[len(staged)])
            all_of(down_w.at[1], down_recv)
        hidden_copy(c).wait_recv()
        total = jnp.dot(hidden_ref[c, 0], down_w[0], preferred_element_type=F32) + jnp.dot(
            hidden_ref[c, 1], down_w[1], preferred_element_type=F32
        )
        for j in range(ny):
            partial[c, j] = total[:, j * LANES : (j + 1) * LANES]

    def reduce_right(c, s):
        return remote(
            send_right.at[c, s],
            recv_right.at[c, s],
            reduce_right_send,
            reduce_right_recv.at[c, s],
            tp=at_y(1) * 2 + core,
        )

    def reduce_left(c, s):
        return remote(
            send_left.at[c, s],
            recv_left.at[c, s],
            reduce_left_send,
            reduce_left_recv.at[c, s],
            tp=at_y(-1) * 2 + core,
        )

    def reduce_step(c, s):
        right, left = reach(c)
        if s < right:
            share = partial[c, at_y(right - s)]
            if s:
                reduce_right(c, s - 1).wait_recv()
                share = share + recv_right[c, s - 1].astype(F32)
            send_right[c, s] = share.astype(BF16)
            reduce_right(c, s).start()
        if s < left:
            share = partial[c, at_y(s - left)]
            if s:
                reduce_left(c, s - 1).wait_recv()
                share = share + recv_left[c, s - 1].astype(F32)
            send_left[c, s] = share.astype(BF16)
            reduce_left(c, s).start()

    def give_back(o):
        dz, dx = offsets[o]
        c, g = divmod(o, per_chunk)
        return remote(
            result_out.at[c, g],
            result_in.at[o],
            return_send,
            return_recv.at[c],
            sp=at_sp(-dz, -dx),
        )

    own_result = pltpu.make_async_copy(
        result_out.at[own_chunk, 0], result_in.at[own], own_result_sem
    )

    def reduce_last(c):
        right, left = reach(c)
        total = partial[c, y]
        if right:
            reduce_right(c, right - 1).wait_recv()
            total = total + recv_right[c, right - 1].astype(F32)
        if left:
            reduce_left(c, left - 1).wait_recv()
            total = total + recv_left[c, left - 1].astype(F32)
        result_out[c] = total.reshape(per_chunk, cap, LANES).astype(BF16)
        for g in range(per_chunk):
            if c * per_chunk + g == own:
                own_result.start()
            else:
                give_back(c * per_chunk + g).start()

    hops = ny // 2
    steps = {
        "start": gather_start,
        "hop": gather_hop,
        "gate": gate_up,
        "down": down_sum,
        "add": reduce_step,
        "last": reduce_last,
    }
    for step in schedule(chunks, hops):
        steps[step[0]](*step[1:])

    blended = [jnp.zeros((tokens, LANES), F32), jnp.zeros((tokens, LANES), F32)]
    for c in range(chunks):
        if c == own_chunk:
            own_result.wait()
        alone = 1 if c == own_chunk else 0
        if alone < per_chunk:
            all_of(
                result_in.at[c * per_chunk + alone : (c + 1) * per_chunk], return_recv.at[c]
            )
        result = (
            result_in[c * per_chunk : (c + 1) * per_chunk]
            .astype(F32)
            .reshape(rows, LANES)
            .astype(BF16)
        )
        at = lax.broadcasted_iota(jnp.int32, (tokens, rows), 1) + c * rows
        for k in range(2):
            choose = jnp.where(at.astype(F32) == slot_cols[k], 1.0, 0.0).astype(BF16)
            blended[k] = blended[k] + jnp.dot(choose, result, preferred_element_type=F32)
    out_ref[...] = (
        stream_ref[...] + weight_cols[0] * blended[0] + weight_cols[1] * blended[1]
    ).astype(out_ref.dtype)

    for copy in halo:
        copy.wait_send()
    all_of(proj_w.at[: (ntp - 1) * channels], proj_send)
    all_of(down_w.at[1], down_send)
    all_of(edge_in.at[: ntp - 1], edge_send)
    all_of(mixed_all.at[: mixed_reach[0] * channels], mixed_right_send)
    all_of(mixed_all.at[: mixed_reach[1] * channels], mixed_left_send)
    all_of(mixed_all.at[: ny * channels], mixed_core_send)
    all_of(packed.at[1:], scatter_send)
    all_of(result_in.at[1:], return_send)
    long = sum(reach(c)[0] for c in range(chunks))
    short = sum(reach(c)[1] for c in range(chunks))
    deep = max(1, chunks // 4)
    all_of(rows_in.at[:deep, : long // deep], gather_right_send)
    all_of(rows_in.at[:deep, : long // deep], reduce_right_send)
    all_of(rows_in.at[:deep, : short // deep], gather_left_send)
    all_of(rows_in.at[:deep, : short // deep], reduce_left_send)
    all_of(rows_in.at[: chunks // 2], gather_core_send)
    all_of(hidden_ref.at[:, 0], hidden_send)


def layer(
    sizes,
    in_gate,
    out_gate,
    values,
    conv_taps,
    doc_ids,
    residual,
    out_weight,
    norm_gain,
    routes,
    route_weights,
    expert_gate,
    expert_up,
    expert_down,
):
    nz, nx, ny, cap, chunks = sizes
    nsp, ntp = nz * nx, 2 * ny
    per_chunk = nsp // chunks
    rows = per_chunk * cap
    tokens = doc_ids.shape[0]
    channels = in_gate.shape[0]
    units = expert_down.shape[1]
    hops = ny // 2
    vmem = pl.BlockSpec(memory_space=pltpu.VMEM)
    hbm = pl.BlockSpec(memory_space=pl.ANY)
    dma = pltpu.SemaphoreType.DMA
    return pl.pallas_call(
        functools.partial(layer_kernel, sizes),
        out_shape=jax.ShapeDtypeStruct((tokens, LANES), BF16),
        in_specs=[hbm] * 13,
        out_specs=vmem,
        scratch_shapes=[
            pltpu.VMEM((channels, tokens), BF16),
            pltpu.VMEM((channels, tokens), BF16),
            pltpu.VMEM((channels, tokens), BF16),
            pltpu.VMEM((3, channels), BF16),
            pltpu.VMEM((1, tokens), jnp.int32),
            pltpu.VMEM((channels, ntp * LANES), BF16),
            pltpu.VMEM((ntp, LANES), BF16),
            pltpu.VMEM((2, tokens), jnp.int32),
            pltpu.VMEM((2, tokens), F32),
            pltpu.VMEM((units, ntp * LANES), BF16),
            pltpu.VMEM((units, ntp * LANES), BF16),
            pltpu.VMEM((2, units, ny * LANES), BF16),
            pltpu.VMEM((tokens, LANES), BF16),
            pltpu.VMEM((channels, LANES), BF16),
            pltpu.VMEM((channels, LANES), BF16),
            pltpu.VMEM((1, LANES), jnp.int32),
            pltpu.VMEM((ntp * channels, tokens), BF16),
            pltpu.VMEM((ntp * channels, LANES), BF16),
            pltpu.VMEM((ntp, 8, LANES), F32),
            pltpu.VMEM((ntp, 8, LANES), F32),
            pltpu.VMEM((tokens, LANES), F32),
            pltpu.VMEM((nsp * cap, tokens), BF16),
            pltpu.VMEM((2, tokens, 1), F32),
            pltpu.VMEM((2, tokens, 1), F32),
            pltpu.VMEM((nsp, cap, LANES), BF16),
            pltpu.VMEM((chunks, ntp, per_chunk, cap, LANES), BF16),
            pltpu.VMEM((rows, ntp * LANES), BF16),
            pltpu.VMEM((chunks, 2, rows, units), BF16),
            pltpu.VMEM((chunks, ny, rows, LANES), F32),
            pltpu.VMEM((chunks, hops, rows, LANES), BF16),
            pltpu.VMEM((chunks, hops, rows, LANES), BF16),
            pltpu.VMEM((chunks, hops, rows, LANES), BF16),
            pltpu.VMEM((chunks, hops, rows, LANES), BF16),
            pltpu.VMEM((chunks, per_chunk, cap, LANES), BF16),
            pltpu.VMEM((nsp, cap, LANES), BF16),
            dma((13,)),
            dma((3,)),
            dma((3,)),
            dma,
            dma,
            dma,
            dma,
            dma,
            dma((hops,)),
            dma,
            dma((hops,)),
            dma,
            dma,
            dma,
            dma,
            dma,
            dma((chunks,)),
            dma,
            dma,
            dma((chunks, hops)),
            dma,
            dma((chunks, hops)),
            dma,
            dma((chunks,)),
            dma,
            dma((chunks,)),
            dma,
            dma((chunks, hops)),
            dma,
            dma((chunks, hops)),
            dma,
            dma((chunks,)),
            dma,
        ],
        compiler_params=pltpu.CompilerParams(
            collective_id=0, has_side_effects=True, vmem_limit_bytes=60 * 1024 * 1024
        ),
        name="layer",
    )(
        in_gate,
        out_gate,
        values,
        conv_taps,
        doc_ids.reshape(1, tokens),
        out_weight,
        norm_gain.reshape(-1, LANES),
        routes.T,
        route_weights.T,
        residual,
        jnp.swapaxes(expert_gate, 1, 2)[0],
        jnp.swapaxes(expert_up, 1, 2)[0],
        expert_down[0],
    )


def solution(mesh):
    placed = (
        P("tp", "sp"),
        P("tp", "sp"),
        P("tp", "sp"),
        P(None, "tp"),
        P("sp"),
        P("sp", None),
        P("tp", None),
        P(),
        P("sp", None),
        P("sp", None),
        P("sp", None, "tp"),
        P("sp", None, "tp"),
        P("sp", "tp", None),
    )
    sizes = (mesh.shape["sp"] // 4, 4, mesh.shape["tp"] // 2, 24, 4)
    return jax.shard_map(
        functools.partial(layer, sizes),
        mesh=mesh,
        in_specs=placed,
        out_specs=P("sp", "tp"),
        check_vma=False,
    )
```

time: 103 us -> 88 us (0.85)
  the two profiles are of different devices: /device:TPU:8 before, /device:TPU:2 now
where the time goes in v2:
time: 88 us; the launch traced here: 87.8 us
  Pallas kernels  86.4 us (98%)
  local copies, waits for them, and re-layouts  1.47 us (2%)
    pallas_call x1, Pallas kernels, layer(): pl.pallas_call(functools.partial(layer_kernel, sizes), out_shape=jax.Shap...  86.4 us

profile of v2, /device:TPU:2, one launch (start us, length us, event | category | flops | bytes accessed | tf_op | source)
XLA Modules:
  0.0 87.8 jit_solution(4768380622940810289)
XLA Ops:
  0.0 86.4 %layer.1 = bf16[256,128]{1,0:T(8,128)(2,1)} custom-call(bf16[64,256]{1,0:T(8,128)(2,1)} %in_gate_hbm.1, bf16[64,256]{1,0:T(8,128)(2,1)} %out_gate_hbm.1, bf16[64,256]{1,0:T(8,128)(2,1)} %values_hbm.1, bf16[3,64]{1,0:T(4,128)(2,1)} %taps_hbm.1, s32[1,256]{1,0:T(1,128)} %bitcast.17, bf16[64,2048]{1,0:T(8,128)(2,1)} %out_weight_hbm.1, ...), custom_call_target="tpu_custom_call" | custom-call | tf_op jit(solution)/shard_map/layer/pallas_call | solution.py:686
  86.4 1.5 %copy.15 = bf16[256,128]{1,0:T(8,128)(2,1)} copy(bf16[256,128]{1,0:T(8,128)(2,1)} %layer.1) | data formatting | bytes 131072

commit v3 on v2

--- a/solution.py
+++ b/solution.py
@@ -21,20 +21,22 @@
 def schedule(chunks, hops):
     steps = [("start", c) for c in range(chunks)]
     for h in range(1, hops):
-        steps += [("hop", c, h) for c in range(chunks)]
+        for c in range(chunks):
+            steps += [("hop", c, h), ("acc", c, h - 1)]
     early = chunks // 2
     for c in range(chunks + 2):
         if c < chunks:
-            steps += [("hop", c, hops)]
+            steps += [("hop", c, hops), ("acc", c, hops - 1)]
         if 0 <= c - 1 < chunks:
-            steps += [("gate", c - 1)]
+            steps += [("acc", c - 1, hops), ("gate", c - 1)]
         if 0 <= c - 2 < chunks:
             steps += [("down", c - 2), ("add", c - 2, 0)]
             if c - 2 >= early:
                 steps += [("add", c - 2 - early, 1)]
+    far_first = (1, 2, 0, 3) if chunks == 4 else range(chunks)
     for s in range(1, hops):
-        steps += [("add", c, s) for c in range(chunks) if s > 1 or c >= chunks - early]
-    return steps + [("last", c) for c in range(chunks)]
+        steps += [("add", c, s) for c in far_first if s > 1 or c >= chunks - early]
+    return steps + [("last", c) for c in far_first]
 
 
 def layer_kernel(
@@ -79,7 +81,11 @@
     weight_cols,
     packed,
     rows_in,
-    normed,
+    squares,
+    gate_sum,
+    up_sum,
+    scale_rows,
+    unscale_rows,
     hidden_ref,
     partial,
     send_right,
@@ -95,10 +101,10 @@
     proj_recv,
     edge_send,
     edge_recv,
-    mixed_right_send,
-    mixed_right_recv,
-    mixed_left_send,
-    mixed_left_recv,
+    along_send,
+    along_recv,
+    mixed_send,
+    mixed_recv,
     mixed_core_send,
     mixed_core_recv,
     down_send,
@@ -129,6 +135,7 @@
     tokens = out_ref.shape[0]
     channels = in_gate.shape[0]
     model_width = ntp * LANES
+    quarter = channels // nx
     order = dz_order(nz)
     offsets = [(dz, dx) for dz in order for dx in range(nx)]
     others = [o for o in range(nsp) if offsets[o] != (0, 0)]
@@ -181,6 +188,13 @@
         (out_weight_hbm, out_weight),
         (out_gate_hbm, out_gate),
         (taps_hbm, taps),
+        (
+            out_weight_hbm.at[
+                pl.ds(pl.multiple_of(x * quarter, quarter), quarter),
+                pl.ds(pl.multiple_of(tp * LANES, LANES), LANES),
+            ],
+            proj_w.at[tp, x],
+        ),
         (residual_hbm.at[:, pl.ds(pl.multiple_of(tp * LANES, LANES), LANES)], residual_cols),
         (gain_hbm, gain),
         (gate_hbm, gate_w),
@@ -247,7 +261,7 @@
         )
         return out.astype(F32) * convolved
 
-    for copy in staged[2:8]:
+    for copy in staged[2:9]:
         copy.wait()
     gated = (in_gate[...].astype(F32) * values[...].astype(F32)).astype(BF16).astype(F32)
     doc_here = jnp.broadcast_to(docs[...].astype(F32), (8, tokens))
@@ -269,7 +283,6 @@
     mixed_all[weight_rows(tp), :] = jnp.where(
         lane < 2, 0.0, convolve(gated, doc_here, rolled, out_gate[...])
     ).astype(BF16)
-    proj_w[weight_rows(tp), :] = out_weight[:, pl.ds(pl.multiple_of(tp * LANES, LANES), LANES)]
 
     pl.semaphore_wait(barrier, nsp - 1 + ntp - 1)
 
@@ -283,50 +296,32 @@
     for copy in halo:
         copy.start()
 
-    mixed_reach = (ny // 2, ny - 1 - ny // 2)
-
-    def mixed_right(h):
-        ref = mixed_all.at[weight_rows(at_y(-h) * 2 + core)]
-        at = mixed_right_recv.at[h]
-        return remote(ref, ref, mixed_right_send, at, tp=at_y(1) * 2 + core)
-
-    def mixed_left(h):
-        ref = mixed_all.at[weight_rows(at_y(h) * 2 + core)]
-        at = mixed_left_recv.at[h]
-        return remote(ref, ref, mixed_left_send, at, tp=at_y(-1) * 2 + core)
-
-    def mixed_core(dy):
-        ref = mixed_all.at[weight_rows(at_y(dy) * 2 + core)]
-        return remote(ref, ref, mixed_core_send, mixed_core_recv, tp=partner)
-
-    def mixed_arrived(dy, sem):
-        all_of(mixed_all.at[weight_rows(at_y(dy) * 2 + core)], sem)
-
     def proj(to):
         return remote(
-            out_weight.at[:, pl.ds(pl.multiple_of(to * LANES, LANES), LANES)],
-            proj_w.at[weight_rows(tp)],
+            out_weight.at[
+                pl.ds(pl.multiple_of(x * quarter, quarter), quarter),
+                pl.ds(pl.multiple_of(to * LANES, LANES), LANES),
+            ],
+            proj_w.at[tp, x],
             proj_send,
             proj_recv,
             tp=to,
         )
 
-    def mixed_hop(h):
-        right, left = mixed_reach
-        if h <= right:
-            if h:
-                mixed_arrived(-h, mixed_right_recv.at[h - 1])
-            if h < right:
-                mixed_right(h).start()
-        if h <= left:
-            if h:
-                mixed_arrived(h, mixed_left_recv.at[h - 1])
-            if h < left:
-                mixed_left(h).start()
-        if h <= right:
-            mixed_core(-h).start()
-        if h and h <= left:
-            mixed_core(h).start()
+    def proj_along(dx):
+        ref = proj_w.at[:, x]
+        return remote(ref, ref, along_send, along_recv, sp=at_sp(0, dx))
+
+    def mixed_rows(dy):
+        return mixed_all.at[weight_rows(at_y(dy) * 2 + core)]
+
+    def mixed_out(dy):
+        ref = mixed_rows(0)
+        return remote(ref, ref, mixed_send, mixed_recv.at[dy], tp=at_y(dy) * 2 + core)
+
+    def mixed_core(dy):
+        ref = mixed_rows(dy)
+        return remote(ref, ref, mixed_core_send, mixed_core_recv, tp=partner)
 
     def edge(to):
         return remote(edge_out.at[to], edge_in.at[tp], edge_send, edge_recv, tp=to)
@@ -366,34 +361,42 @@
         edge_in[tp] = edge_out[tp]
 
     distances = sorted(range(1, ny), key=lambda d: -min(d, ny - d))
-    batches = [distances[i : i + 2] for i in range(0, len(distances), 2)]
-    for h in range(max(mixed_reach) + 1):
-        mixed_hop(h)
-        if h == 0:
-            proj(partner).start()
-        if h < len(batches):
-            for d in batches[h]:
-                proj(at_y(d) * 2 + core).start()
-                proj(at_y(d) * 2 + other).start()
-        if h == min(2, max(mixed_reach)):
-            edge_rows()
-    for h in range(max(mixed_reach) + 1, len(batches)):
-        for d in batches[h]:
-            proj(at_y(d) * 2 + core).start()
-            proj(at_y(d) * 2 + other).start()
-    all_of(proj_w.at[: (ntp - 1) * channels], proj_recv)
-    staged[8].wait()
+    for d in distances:
+        proj(at_y(d) * 2 + core).start()
+        proj(at_y(d) * 2 + other).start()
+    proj(partner).start()
+    for d in distances:
+        mixed_out(d).start()
+    mixed_core(0).start()
+    all_of(proj_w.at[: ntp - 1, 0], proj_recv)
+    for dx in range(1, nx):
+        proj_along(dx).start()
+    edge_rows()
+    for d in distances:
+        all_of(mixed_rows(-d), mixed_recv.at[d])
+        mixed_core(-d).start()
+    if nx > 1:
+        all_of(proj_w.at[:, : nx - 1], along_recv)
+    staged[9].wait()
+    staged[10].wait()
+    for b in range(ntp):
+        row = gain[b : b + 1, :].astype(F32)
+        scale_rows[b] = jnp.broadcast_to(row, (8, LANES))
+        unscale_rows[b] = jnp.broadcast_to(1.0 / row, (8, LANES))
     all_of(mixed_all.at[: ny * channels], mixed_core_recv)
     projected = lax.dot_general(
-        mixed_all[...], proj_w[...], (((0,), (0,)), ((), ())), preferred_element_type=F32
+        mixed_all[...],
+        proj_w[...].reshape(ntp * channels, LANES),
+        (((0,), (0,)), ((), ())), preferred_element_type=F32
     )
     stream_ref[...] = residual_cols[...].astype(F32) + projected
     all_of(edge_in.at[: ntp - 1], edge_recv)
     stream_ref[:8, :] = stream_ref[:8, :] + jnp.sum(edge_in[...], axis=0)
     stream = stream_ref[...]
 
+    scaled = stream * scale_rows[tp][0:1, :]
     packed[...] = (
-        jnp.dot(pick_ref[...], stream.astype(BF16), preferred_element_type=F32)
+        jnp.dot(pick_ref[...], scaled.astype(BF16), preferred_element_type=F32)
         .reshape(nsp, cap, LANES)
         .astype(BF16)
     )
@@ -468,7 +471,8 @@
 
     def gather_core(c, dy):
         ref = block(c, at_y(dy), core)
-        return remote(ref, ref, gather_core_send, gather_core_recv.at[c], tp=partner)
+        at = gather_core_recv.at[c, abs(dy)]
+        return remote(ref, ref, gather_core_send, at, tp=partner)
 
     def gather_start(c):
         if c == own_chunk:
@@ -496,26 +500,48 @@
                 gather_left(c, h).start()
             gather_core(c, h).start()
 
+    def accumulate(c, h):
+        right, left = reach(c)
+        chips = [at_y(-h)] if h <= right else []
+        if h and h <= left:
+            chips.append(at_y(h))
+        all_of(rows_in.at[c, : len(chips)], gather_core_recv.at[c, h])
+        if c == 0 and h == 0:
+            staged[11].wait()
+            staged[12].wait()
+        contract = (((1,), (1,)), ((), ()))
+        gates, ups, square = [], [], []
+        for chip in chips:
+            parts = []
+            for k in range(2):
+                part = rows_in[c, chip * 2 + k].astype(F32).reshape(rows, LANES)
+                plain = part * unscale_rows[chip * 2 + k][0:1, :]
+                square.append(plain * plain)
+                parts.append(part.astype(BF16))
+            block = jnp.concatenate(parts, axis=1)
+            features = pl.ds(pl.multiple_of(chip * 2 * LANES, 2 * LANES), 2 * LANES)
+            for weight, sums in ((gate_w, gates), (up_w, ups)):
+                sums.append(
+                    lax.dot_general(
+                        weight[:, features], block, contract, preferred_element_type=F32
+                    )
+                )
+        for ref, terms in ((gate_sum, gates), (up_sum, ups), (squares, square)):
+            if h:
+                terms.append(ref[c])
+            ref[c] = functools.reduce(lambda a, b: a + b, terms)
+
     def gate_up(c):
-        all_of(rows_in.at[c, :ny], gather_core_recv.at[c])
-        if c == 0:
-            for copy in staged[9:]:
-                copy.wait()
-        squares = jnp.zeros((rows, LANES), F32)
-        for b in range(ntp):
-            part = rows_in[c, b].astype(F32).reshape(rows, LANES)
-            squares = squares + part * part
         inverse = lax.rsqrt(
-            jnp.sum(squares, axis=1, keepdims=True) / model_width + EPSILON
-        )
-        for b in range(ntp):
-            at = slice(b * LANES, (b + 1) * LANES)
-            part = rows_in[c, b].astype(F32).reshape(rows, LANES)
-            normed[:, at] = (part * inverse * gain[b : b + 1, :].astype(F32)).astype(BF16)
-        contract = (((1,), (1,)), ((), ()))
-        gate_sum = lax.dot_general(normed[...], gate_w[...], contract, preferred_element_type=F32)
-        up_sum = lax.dot_general(normed[...], up_w[...], contract, preferred_element_type=F32)
-        hidden_ref[c, 0] = (gate_sum / (1.0 + jnp.exp(-gate_sum)) * up_sum).astype(BF16)
+            jnp.sum(squares[c], axis=1, keepdims=True) / model_width + EPSILON
+        )
+        corner = lax.broadcasted_iota(jnp.int32, (rows, rows), 0) == lax.broadcasted_iota(
+            jnp.int32, (rows, rows), 1
+        )
+        inverse = jnp.sum(jnp.where(corner, inverse, 0.0), axis=0, keepdims=True)
+        gate = gate_sum[c] * inverse
+        up = up_sum[c] * inverse
+        hidden_ref[c, 0] = (gate / (1.0 + jnp.exp(-gate)) * up).T.astype(BF16)
         hidden_copy(c).start()
 
     def hidden_copy(c):
@@ -604,6 +630,7 @@
     steps = {
         "start": gather_start,
         "hop": gather_hop,
+        "acc": accumulate,
         "gate": gate_up,
         "down": down_sum,
         "add": reduce_step,
@@ -637,11 +664,12 @@
 
     for copy in halo:
         copy.wait_send()
-    all_of(proj_w.at[: (ntp - 1) * channels], proj_send)
+    all_of(proj_w.at[: ntp - 1, 0], proj_send)
+    if nx > 1:
+        all_of(proj_w.at[:, : nx - 1], along_send)
     all_of(down_w.at[1], down_send)
     all_of(edge_in.at[: ntp - 1], edge_send)
-    all_of(mixed_all.at[: mixed_reach[0] * channels], mixed_right_send)
-    all_of(mixed_all.at[: mixed_reach[1] * channels], mixed_left_send)
+    all_of(mixed_all.at[: (ny - 1) * channels], mixed_send)
     all_of(mixed_all.at[: ny * channels], mixed_core_send)
     all_of(packed.at[1:], scatter_send)
     all_of(result_in.at[1:], return_send)
@@ -685,7 +713,7 @@
     dma = pltpu.SemaphoreType.DMA
     return pl.pallas_call(
         functools.partial(layer_kernel, sizes),
-        out_shape=jax.ShapeDtypeStruct((tokens, LANES), BF16),
+        out_shape=pltpu.VMEM((tokens, LANES), BF16),
         in_specs=[hbm] * 13,
         out_specs=vmem,
         scratch_shapes=[
@@ -706,7 +734,7 @@
             pltpu.VMEM((channels, LANES), BF16),
             pltpu.VMEM((1, LANES), jnp.int32),
             pltpu.VMEM((ntp * channels, tokens), BF16),
-            pltpu.VMEM((ntp * channels, LANES), BF16),
+            pltpu.VMEM((ntp, nx, channels // nx, LANES), BF16),
             pltpu.VMEM((ntp, 8, LANES), F32),
             pltpu.VMEM((ntp, 8, LANES), F32),
             pltpu.VMEM((tokens, LANES), F32),
@@ -715,7 +743,11 @@
             pltpu.VMEM((2, tokens, 1), F32),
             pltpu.VMEM((nsp, cap, LANES), BF16),
             pltpu.VMEM((chunks, ntp, per_chunk, cap, LANES), BF16),
-            pltpu.VMEM((rows, ntp * LANES), BF16),
+            pltpu.VMEM((chunks, rows, LANES), F32),
+            pltpu.VMEM((chunks, units, rows), F32),
+            pltpu.VMEM((chunks, units, rows), F32),
+            pltpu.VMEM((ntp, 8, LANES), F32),
+            pltpu.VMEM((ntp, 8, LANES), F32),
             pltpu.VMEM((chunks, 2, rows, units), BF16),
             pltpu.VMEM((chunks, ny, rows, LANES), F32),
             pltpu.VMEM((chunks, hops, rows, LANES), BF16),
@@ -724,7 +756,7 @@
             pltpu.VMEM((chunks, hops, rows, LANES), BF16),
             pltpu.VMEM((chunks, per_chunk, cap, LANES), BF16),
             pltpu.VMEM((nsp, cap, LANES), BF16),
-            dma((13,)),
+            dma((14,)),
             dma((3,)),
             dma((3,)),
             dma,
@@ -732,9 +764,9 @@
             dma,
             dma,
             dma,
-            dma((hops,)),
-            dma,
-            dma((hops,)),
+            dma,
+            dma,
+            dma((ny,)),
             dma,
             dma,
             dma,
@@ -747,7 +779,7 @@
             dma,
             dma((chunks, hops)),
             dma,
-            dma((chunks,)),
+            dma((chunks, hops + 1)),
             dma,
             dma((chunks,)),
             dma,

time: 88 us -> 80.6 us (0.916)
  the two profiles are of different devices: /device:TPU:2 before, /device:TPU:16 now
where the time goes in v3:
time: 80.6 us; the launch traced here: 80.5 us
  Pallas kernels  79.9 us (99%)
    pallas_call x1, Pallas kernels, layer(): pl.pallas_call(functools.partial(layer_kernel, sizes), out_shape=pltpu.VM...  79.9 us

profile of v3, /device:TPU:16, one launch (start us, length us, event | category | flops | bytes accessed | tf_op | source)
XLA Modules:
  0.0 80.5 jit_solution(15283872017961031516)
XLA Ops:
  0.0 79.9 %layer.1 = bf16[256,128]{1,0:T(8,128)(2,1)S(1)} custom-call(bf16[64,256]{1,0:T(8,128)(2,1)} %in_gate_hbm.1, bf16[64,256]{1,0:T(8,128)(2,1)} %out_gate_hbm.1, bf16[64,256]{1,0:T(8,128)(2,1)} %values_hbm.1, bf16[3,64]{1,0:T(4,128)(2,1)} %taps_hbm.1, s32[1,256]{1,0:T(1,128)} %bitcast.17, bf16[64,2048]{1,0:T(8,128)(2,1)} %out_weight_hbm.1, ...), custom_call_target="tpu_custom_call" | custom-call | tf_op jit(solution)/shard_map/layer/pallas_call | solution.py:714
  79.9 0.6 copy.15

commit v4 on v3

--- a/solution.py
+++ b/solution.py
@@ -23,6 +23,8 @@
     for h in range(1, hops):
         for c in range(chunks):
             steps += [("hop", c, h), ("acc", c, h - 1)]
+        if h == 1:
+            steps += [("share",)]
     early = chunks // 2
     for c in range(chunks + 2):
         if c < chunks:
@@ -127,6 +129,7 @@
     return_send,
     return_recv,
     own_result_sem,
+    row_ready,
 ):
     nz, nx, ny, cap, chunks = sizes
     nsp, ntp = nz * nx, 2 * ny
@@ -170,14 +173,12 @@
         pltpu.make_async_copy(ref, ref, sem).wait()
 
     barrier = pltpu.get_barrier_semaphore()
-    for d in range(1, nsp):
-        pl.semaphore_signal(
-            barrier, inc=1, device_id={"sp": (sp + d) % nsp}, device_id_type=MESH
-        )
-    for d in range(1, ntp):
-        pl.semaphore_signal(
-            barrier, inc=1, device_id={"tp": (tp + d) % ntp}, device_id_type=MESH
-        )
+    near = [{"tp": (tp + d) % ntp} for d in range(1, ntp)]
+    near += [{"sp": at_sp(0, d)} for d in range(1, nx)]
+    near += [{"sp": at_sp(d, 0)} for d in range(1, nz)]
+    near += [{"sp": (sp + d) % nsp} for d in (1, nsp - 1)]
+    for where in near:
+        pl.semaphore_signal(barrier, inc=1, device_id=where, device_id_type=MESH)
 
     staged = [
         (routes_hbm, routes_t),
@@ -284,7 +285,11 @@
         lane < 2, 0.0, convolve(gated, doc_here, rolled, out_gate[...])
     ).astype(BF16)
 
-    pl.semaphore_wait(barrier, nsp - 1 + ntp - 1)
+    pl.semaphore_wait(barrier, len(near))
+    for d in range(1, nx):
+        pl.semaphore_signal(
+            row_ready, inc=1, device_id={"sp": at_sp(0, d)}, device_id_type=MESH
+        )
 
     after = (sp + 1) % nsp
     last = slice(tokens - LANES, tokens)
@@ -368,10 +373,10 @@
     for d in distances:
         mixed_out(d).start()
     mixed_core(0).start()
+    edge_rows()
     all_of(proj_w.at[: ntp - 1, 0], proj_recv)
     for dx in range(1, nx):
         proj_along(dx).start()
-    edge_rows()
     for d in distances:
         all_of(mixed_rows(-d), mixed_recv.at[d])
         mixed_core(-d).start()
@@ -395,12 +400,6 @@
     stream = stream_ref[...]
 
     scaled = stream * scale_rows[tp][0:1, :]
-    packed[...] = (
-        jnp.dot(pick_ref[...], scaled.astype(BF16), preferred_element_type=F32)
-        .reshape(nsp, cap, LANES)
-        .astype(BF16)
-    )
-
     def scatter(o):
         dz, dx = offsets[o]
         c, g = divmod(o, per_chunk)
@@ -413,18 +412,22 @@
         )
 
     own_rows = pltpu.make_async_copy(packed.at[own], rows_in.at[own_chunk, tp, 0], own_sem)
-    own_rows.start()
-    for o in others:
-        scatter(o).start()
-
-    for j in range(ny):
-        remote(
-            down_hbm.at[:, pl.ds(pl.multiple_of((2 * j + other) * LANES, LANES), LANES)],
-            down_w.at[1, :, j * LANES : (j + 1) * LANES],
-            down_send,
-            down_recv,
-            tp=partner,
-        ).start()
+    scaled = scaled.astype(BF16)
+    if nx > 1:
+        pl.semaphore_wait(row_ready, nx - 1)
+    for c in range(chunks):
+        packed[c * per_chunk : (c + 1) * per_chunk] = (
+            jnp.dot(
+                pick_ref[c * rows : (c + 1) * rows, :], scaled, preferred_element_type=F32
+            )
+            .reshape(per_chunk, cap, LANES)
+            .astype(BF16)
+        )
+        for o in range(c * per_chunk, (c + 1) * per_chunk):
+            if o == own:
+                own_rows.start()
+            else:
+                scatter(o).start()
 
     def reach(c):
         long, short = ny // 2, ny - 1 - ny // 2
@@ -544,6 +547,16 @@
         hidden_ref[c, 0] = (gate / (1.0 + jnp.exp(-gate)) * up).T.astype(BF16)
         hidden_copy(c).start()
 
+    def share_down():
+        for j in range(ny):
+            remote(
+                down_hbm.at[:, pl.ds(pl.multiple_of((2 * j + other) * LANES, LANES), LANES)],
+                down_w.at[1, :, j * LANES : (j + 1) * LANES],
+                down_send,
+                down_recv,
+                tp=partner,
+            ).start()
+
     def hidden_copy(c):
         return remote(
             hidden_ref.at[c, 0], hidden_ref.at[c, 1], hidden_send, hidden_recv.at[c], tp=partner
@@ -631,6 +644,7 @@
         "start": gather_start,
         "hop": gather_hop,
         "acc": accumulate,
+        "share": share_down,
         "gate": gate_up,
         "down": down_sum,
         "add": reduce_step,
@@ -789,6 +803,7 @@
             dma,
             dma((chunks,)),
             dma,
+            pltpu.SemaphoreType.REGULAR,
         ],
         compiler_params=pltpu.CompilerParams(
             collective_id=0, has_side_effects=True, vmem_limit_bytes=60 * 1024 * 1024

time: 80.6 us -> 79.3 us (0.984)
  the two profiles are of different devices: /device:TPU:16 before, /device:TPU:2 now
where the time goes in v4:
time: 79.3 us; the launch traced here: 79.2 us
  Pallas kernels  78.6 us (99%)
    pallas_call x1, Pallas kernels, layer(): pl.pallas_call(functools.partial(layer_kernel, sizes), out_shape=pltpu.VM...  78.6 us

profile of v4, /device:TPU:2, one launch (start us, length us, event | category | flops | bytes accessed | tf_op | source)
XLA Modules:
  0.0 79.2 jit_solution(12557256927204166015)
XLA Ops:
  0.0 78.6 %layer.1 = bf16[256,128]{1,0:T(8,128)(2,1)S(1)} custom-call(bf16[64,256]{1,0:T(8,128)(2,1)} %in_gate_hbm.1, bf16[64,256]{1,0:T(8,128)(2,1)} %out_gate_hbm.1, bf16[64,256]{1,0:T(8,128)(2,1)} %values_hbm.1, bf16[3,64]{1,0:T(4,128)(2,1)} %taps_hbm.1, s32[1,256]{1,0:T(1,128)} %bitcast.17, bf16[64,2048]{1,0:T(8,128)(2,1)} %out_weight_hbm.1, ...), custom_call_target="tpu_custom_call" | custom-call | tf_op jit(solution)/shard_map/layer/pallas_call | solution.py:728
  78.6 0.6 copy.15

commit v5 on v4

--- a/solution.py
+++ b/solution.py
@@ -25,7 +25,6 @@
             steps += [("hop", c, h), ("acc", c, h - 1)]
         if h == 1:
             steps += [("share",)]
-    early = chunks // 2
     for c in range(chunks + 2):
         if c < chunks:
             steps += [("hop", c, hops), ("acc", c, hops - 1)]
@@ -33,11 +32,9 @@
             steps += [("acc", c - 1, hops), ("gate", c - 1)]
         if 0 <= c - 2 < chunks:
             steps += [("down", c - 2), ("add", c - 2, 0)]
-            if c - 2 >= early:
-                steps += [("add", c - 2 - early, 1)]
     far_first = (1, 2, 0, 3) if chunks == 4 else range(chunks)
     for s in range(1, hops):
-        steps += [("add", c, s) for c in far_first if s > 1 or c >= chunks - early]
+        steps += [("add", c, s) for c in far_first]
     return steps + [("last", c) for c in far_first]
 
 
@@ -135,6 +132,7 @@
     nsp, ntp = nz * nx, 2 * ny
     per_chunk = nsp // chunks
     rows = per_chunk * cap
+    hops = ny // 2
     tokens = out_ref.shape[0]
     channels = in_gate.shape[0]
     model_width = ntp * LANES
@@ -173,12 +171,22 @@
         pltpu.make_async_copy(ref, ref, sem).wait()
 
     barrier = pltpu.get_barrier_semaphore()
+    after = (sp + 1) % nsp
     near = [{"tp": (tp + d) % ntp} for d in range(1, ntp)]
     near += [{"sp": at_sp(0, d)} for d in range(1, nx)]
     near += [{"sp": at_sp(d, 0)} for d in range(1, nz)]
-    near += [{"sp": (sp + d) % nsp} for d in (1, nsp - 1)]
     for where in near:
         pl.semaphore_signal(barrier, inc=1, device_id=where, device_id_type=MESH)
+
+    @pl.when(sp < nsp - 1)
+    def _():
+        pl.semaphore_signal(barrier, inc=1, device_id={"sp": after}, device_id_type=MESH)
+
+    @pl.when(sp > 0)
+    def _():
+        pl.semaphore_signal(
+            barrier, inc=1, device_id={"sp": (sp + nsp - 1) % nsp}, device_id_type=MESH
+        )
 
     staged = [
         (routes_hbm, routes_t),
@@ -285,21 +293,24 @@
         lane < 2, 0.0, convolve(gated, doc_here, rolled, out_gate[...])
     ).astype(BF16)
 
-    pl.semaphore_wait(barrier, len(near))
+    pl.semaphore_wait(barrier, len(near) + (sp + nsp - 1) // nsp + 1 - sp // (nsp - 1))
     for d in range(1, nx):
         pl.semaphore_signal(
             row_ready, inc=1, device_id={"sp": at_sp(0, d)}, device_id_type=MESH
         )
 
-    after = (sp + 1) % nsp
     last = slice(tokens - LANES, tokens)
     halo = [
         remote(in_gate.at[:, last], halo_gate, halo_send.at[0], halo_recv.at[0], sp=after),
         remote(values.at[:, last], halo_values, halo_send.at[1], halo_recv.at[1], sp=after),
         remote(docs.at[:, last], halo_docs, halo_send.at[2], halo_recv.at[2], sp=after),
     ]
-    for copy in halo:
-        copy.start()
+
+    @pl.when(sp < nsp - 1)
+    def _():
+        for copy in halo:
+            copy.start()
+
 
     def proj(to):
         return remote(
@@ -332,8 +343,16 @@
         return remote(edge_out.at[to], edge_in.at[tp], edge_send, edge_recv, tp=to)
 
     def edge_rows():
-        for copy in halo:
-            copy.wait_recv()
+        @pl.when(sp > 0)
+        def _():
+            for copy in halo:
+                copy.wait_recv()
+
+        @pl.when(sp == 0)
+        def _():
+            for ref in (halo_gate, halo_values, halo_docs):
+                ref[...] = jnp.zeros_like(ref)
+
         before_edge = (
             (halo_gate[...].astype(F32) * halo_values[...].astype(F32)).astype(BF16).astype(F32)
         )
@@ -567,11 +586,24 @@
             all_of(down_w.at[0], local_sem.at[len(staged)])
             all_of(down_w.at[1], down_recv)
         hidden_copy(c).wait_recv()
-        total = jnp.dot(hidden_ref[c, 0], down_w[0], preferred_element_type=F32) + jnp.dot(
-            hidden_ref[c, 1], down_w[1], preferred_element_type=F32
-        )
-        for j in range(ny):
-            partial[c, j] = total[:, j * LANES : (j + 1) * LANES]
+        share(c, 0)
+
+    def share(c, s):
+        right, left = reach(c)
+        blocks = [
+            pl.ds(pl.multiple_of(chip * LANES, LANES), LANES)
+            for chip in (at_y(right - s), at_y(s - left))
+        ]
+        total = sum(
+            jnp.dot(
+                hidden_ref[c, k],
+                jnp.concatenate([down_w[k, :, at] for at in blocks], axis=1),
+                preferred_element_type=F32,
+            )
+            for k in range(2)
+        )
+        partial[c, 0] = total[:, :LANES]
+        partial[c, 1] = total[:, LANES:]
 
     def reduce_right(c, s):
         return remote(
@@ -593,20 +625,24 @@
 
     def reduce_step(c, s):
         right, left = reach(c)
+        if s == 1:
+            share(c, 1)
         if s < right:
-            share = partial[c, at_y(right - s)]
+            total = partial[c, 0]
             if s:
                 reduce_right(c, s - 1).wait_recv()
-                share = share + recv_right[c, s - 1].astype(F32)
-            send_right[c, s] = share.astype(BF16)
+                total = total + recv_right[c, s - 1].astype(F32)
+            send_right[c, s] = total.astype(BF16)
             reduce_right(c, s).start()
         if s < left:
-            share = partial[c, at_y(s - left)]
+            total = partial[c, 1]
             if s:
                 reduce_left(c, s - 1).wait_recv()
-                share = share + recv_left[c, s - 1].astype(F32)
-            send_left[c, s] = share.astype(BF16)
+                total = total + recv_left[c, s - 1].astype(F32)
+            send_left[c, s] = total.astype(BF16)
             reduce_left(c, s).start()
+        if s and s + 1 < hops:
+            share(c, s + 1)
 
     def give_back(o):
         dz, dx = offsets[o]
@@ -625,7 +661,7 @@
 
     def reduce_last(c):
         right, left = reach(c)
-        total = partial[c, y]
+        total = partial[c, 0 if right < left else 1]
         if right:
             reduce_right(c, right - 1).wait_recv()
             total = total + recv_right[c, right - 1].astype(F32)
@@ -639,7 +675,6 @@
             else:
                 give_back(c * per_chunk + g).start()
 
-    hops = ny // 2
     steps = {
         "start": gather_start,
         "hop": gather_hop,
@@ -676,8 +711,11 @@
         stream_ref[...] + weight_cols[0] * blended[0] + weight_cols[1] * blended[1]
     ).astype(out_ref.dtype)
 
-    for copy in halo:
-        copy.wait_send()
+    @pl.when(sp < nsp - 1)
+    def _():
+        for copy in halo:
+            copy.wait_send()
+
     all_of(proj_w.at[: ntp - 1, 0], proj_send)
     if nx > 1:
         all_of(proj_w.at[:, : nx - 1], along_send)
@@ -763,7 +801,7 @@
             pltpu.VMEM((ntp, 8, LANES), F32),
             pltpu.VMEM((ntp, 8, LANES), F32),
             pltpu.VMEM((chunks, 2, rows, units), BF16),
-            pltpu.VMEM((chunks, ny, rows, LANES), F32),
+            pltpu.VMEM((chunks, 2, rows, LANES), F32),
             pltpu.VMEM((chunks, hops, rows, LANES), BF16),
             pltpu.VMEM((chunks, hops, rows, LANES), BF16),
             pltpu.VMEM((chunks, hops, rows, LANES), BF16),

time: 79.3 us -> 78.8 us (level)
  the two profiles are of different devices: /device:TPU:2 before, /device:TPU:16 now
where the time goes in v5:
time: 78.8 us; the launch traced here: 78.6 us
  Pallas kernels  78 us (99%)
    pallas_call x1, Pallas kernels, layer(): pl.pallas_call(functools.partial(layer_kernel, sizes), out_shape=pltpu.VM...  78 us

profile of v5, /device:TPU:16, one launch (start us, length us, event | category | flops | bytes accessed | tf_op | source)
XLA Modules:
  0.0 78.6 jit_solution(13692236300708027180)
XLA Ops:
  0.0 78.0 %layer.1 = bf16[256,128]{1,0:T(8,128)(2,1)S(1)} custom-call(bf16[64,256]{1,0:T(8,128)(2,1)} %in_gate_hbm.1, bf16[64,256]{1,0:T(8,128)(2,1)} %out_gate_hbm.1, bf16[64,256]{1,0:T(8,128)(2,1)} %values_hbm.1, bf16[3,64]{1,0:T(4,128)(2,1)} %taps_hbm.1, s32[1,256]{1,0:T(1,128)} %bitcast.17, bf16[64,2048]{1,0:T(8,128)(2,1)} %out_weight_hbm.1, ...), custom_call_target="tpu_custom_call" | custom-call | tf_op jit(solution)/shard_map/layer/pallas_call | solution.py:766
  78.0 0.6 copy.15

commit v6 on v5

--- a/solution.py
+++ b/solution.py
@@ -112,17 +112,15 @@
     scatter_recv,
     own_sem,
     gather_right_send,
-    gather_right_recv,
+    gather_recv,
     gather_left_send,
-    gather_left_recv,
     gather_core_send,
     gather_core_recv,
     hidden_send,
     hidden_recv,
     reduce_right_send,
-    reduce_right_recv,
+    reduce_recv,
     reduce_left_send,
-    reduce_left_recv,
     return_send,
     return_recv,
     own_result_sem,
@@ -461,34 +459,14 @@
             ref,
             ref,
             gather_right_send,
-            gather_right_recv.at[c, h],
+            gather_recv.at[c, h],
             tp=at_y(1) * 2 + core,
         )
 
     def gather_left(c, h):
         ref = block(c, at_y(h), core)
         return remote(
-            ref, ref, gather_left_send, gather_left_recv.at[c, h], tp=at_y(-1) * 2 + core
-        )
-
-    def arrived_right(c, h):
-        ref = block(c, at_y(-h), core)
-        return remote(
-            ref,
-            ref,
-            gather_right_send,
-            gather_right_recv.at[c, h - 1],
-            tp=at_y(1) * 2 + core,
-        )
-
-    def arrived_left(c, h):
-        ref = block(c, at_y(h), core)
-        return remote(
-            ref,
-            ref,
-            gather_left_send,
-            gather_left_recv.at[c, h - 1],
-            tp=at_y(-1) * 2 + core,
+            ref, ref, gather_left_send, gather_recv.at[c, h], tp=at_y(-1) * 2 + core
         )
 
     def gather_core(c, dy):
@@ -511,13 +489,12 @@
 
     def gather_hop(c, h):
         right, left = reach(c)
+        all_of(rows_in.at[c, : (h <= right) + (h <= left)], gather_recv.at[c, h - 1])
         if h <= right:
-            arrived_right(c, h).wait_recv()
             if h < right:
                 gather_right(c, h).start()
             gather_core(c, -h).start()
         if h <= left:
-            arrived_left(c, h).wait_recv()
             if h < left:
                 gather_left(c, h).start()
             gather_core(c, h).start()
@@ -610,7 +587,7 @@
             send_right.at[c, s],
             recv_right.at[c, s],
             reduce_right_send,
-            reduce_right_recv.at[c, s],
+            reduce_recv.at[c, s],
             tp=at_y(1) * 2 + core,
         )
 
@@ -619,7 +596,7 @@
             send_left.at[c, s],
             recv_left.at[c, s],
             reduce_left_send,
-            reduce_left_recv.at[c, s],
+            reduce_recv.at[c, s],
             tp=at_y(-1) * 2 + core,
         )
 
@@ -627,17 +604,17 @@
         right, left = reach(c)
         if s == 1:
             share(c, 1)
+        if s:
+            all_of(recv_right.at[c, :2], reduce_recv.at[c, s - 1])
         if s < right:
             total = partial[c, 0]
             if s:
-                reduce_right(c, s - 1).wait_recv()
                 total = total + recv_right[c, s - 1].astype(F32)
             send_right[c, s] = total.astype(BF16)
             reduce_right(c, s).start()
         if s < left:
             total = partial[c, 1]
             if s:
-                reduce_left(c, s - 1).wait_recv()
                 total = total + recv_left[c, s - 1].astype(F32)
             send_left[c, s] = total.astype(BF16)
             reduce_left(c, s).start()
@@ -662,11 +639,14 @@
     def reduce_last(c):
         right, left = reach(c)
         total = partial[c, 0 if right < left else 1]
-        if right:
-            reduce_right(c, right - 1).wait_recv()
+        if right == left - 1:
             total = total + recv_right[c, right - 1].astype(F32)
-        if left:
-            reduce_left(c, left - 1).wait_recv()
+        else:
+            total = total + recv_left[c, left - 1].astype(F32)
+        all_of(recv_right.at[c, 0], reduce_recv.at[c, hops - 1])
+        if right == hops:
+            total = total + recv_right[c, right - 1].astype(F32)
+        if left == hops:
             total = total + recv_left[c, left - 1].astype(F32)
         result_out[c] = total.reshape(per_chunk, cap, LANES).astype(BF16)
         for g in range(per_chunk):
@@ -829,15 +809,13 @@
             dma,
             dma((chunks, hops)),
             dma,
+            dma,
+            dma((chunks, hops + 1)),
+            dma,
+            dma((chunks,)),
+            dma,
             dma((chunks, hops)),
             dma,
-            dma((chunks, hops + 1)),
-            dma,
-            dma((chunks,)),
-            dma,
-            dma((chunks, hops)),
-            dma,
-            dma((chunks, hops)),
             dma,
             dma((chunks,)),
             dma,

time: 78.8 us -> 79.6 us (1.010)
  the two profiles are of different devices: /device:TPU:16 before, /device:TPU:2 now
where the time goes in v6:
time: 79.6 us; the launch traced here: 79.4 us
  Pallas kernels  78.8 us (99%)
    pallas_call x1, Pallas kernels, layer(): pl.pallas_call(functools.partial(layer_kernel, sizes), out_shape=pltpu.VM...  78.8 us

profile of v6, /device:TPU:2, one launch (start us, length us, event | category | flops | bytes accessed | tf_op | source)
XLA Modules:
  0.0 79.4 jit_solution(11044145487029719076)
XLA Ops:
  0.0 78.8 %layer.1 = bf16[256,128]{1,0:T(8,128)(2,1)S(1)} custom-call(bf16[64,256]{1,0:T(8,128)(2,1)} %in_gate_hbm.1, bf16[64,256]{1,0:T(8,128)(2,1)} %out_gate_hbm.1, bf16[64,256]{1,0:T(8,128)(2,1)} %values_hbm.1, bf16[3,64]{1,0:T(4,128)(2,1)} %taps_hbm.1, s32[1,256]{1,0:T(1,128)} %bitcast.17, bf16[64,2048]{1,0:T(8,128)(2,1)} %out_weight_hbm.1, ...), custom_call_target="tpu_custom_call" | custom-call | tf_op jit(solution)/shard_map/layer/pallas_call | solution.py:746
  78.8 0.6 copy.15
